TPU v7x, 32 devices: a whole 2x2x4 slice. The times are simulated.
32 devices in a mesh: fs: 8 (over z, y), tp: 4 (over x, core).
Axes of the slice: x: 2, y: 2, z: 4, core: 2. Of those that a mesh axis runs over, the one named last changes fastest.
Arguments:
- tokens: bfloat16 [1024, 2048], P('fs', 'tp'), may hold values from -6 to 6
- routes: int32 [1024, 2], P('fs'), may hold values from 0 to 7, all different within a row; in each aligned block of 128 rows (0 to 127, 128 to 255, ...) at most 48 rows name the same one
- route_weight: float32 [1024, 2], P('fs'), may hold values from 0.05 to 1
- gain: float32 [2048], P('fs'), may hold values from 0.1 to 1.9
- gate_weight: float32 [8, 2048, 512], P(None, 'fs', 'tp'), may hold values from -0.125 to 0.125
- up_weight: float32 [8, 2048, 512], P(None, 'fs', 'tp'), may hold values from -0.125 to 0.125
- down_weight: float32 [8, 512, 2048], P(None, 'tp', 'fs'), may hold values from -0.25 to 0.25
Outputs:
- gate_out: bfloat16 [8, 2048, 512], P('fs', None, 'tp')
- up_out: bfloat16 [8, 2048, 512], P('fs', None, 'tp')
- down_out: bfloat16 [8, 512, 2048], P('fs', 'tp')
- mixed: bfloat16 [1024, 2048], P('fs', 'tp')
Inputs may be any that keep to these rules, and one draw needn't show every extreme that they name: `routes`: each row names 2 different experts. Among the rows of one index of fs (aligned blocks of 128 rows) no expert is named more than 48 times, a bound that some block reaches.
All inputs are finite; a program needn't handle non-finite values.
Results may differ from a plain program's by a relative error of at most 0.0095.
Values may be sent and summed in bfloat16 or wider, within the bound.
A program may use at most 64 MiB of HBM per device.

v0:
```python
import functools

import jax
import jax.numpy as jnp
from jax import lax
from jax.experimental import pallas as pl
from jax.experimental.pallas import tpu as pltpu
from jax.sharding import PartitionSpec as P


def normalize(rows):
    values = rows.astype(jnp.float32)
    return (values * lax.rsqrt(jnp.mean(values * values, axis=-1, keepdims=True) + 1e-06)).astype(
        jnp.bfloat16
    )


def local(tokens, routes, route_weight, gain, gate_weight, up_weight, down_weight):
    fs_count = lax.axis_size("fs")
    tp_count = lax.axis_size("tp")
    gain_rows = gain[None, :, None]
    gate_new = (gain_rows * gate_weight).astype(jnp.bfloat16)
    up_new = (gain_rows * up_weight).astype(jnp.bfloat16)
    gate_out, up_out = (
        lax.all_to_all(gate_new, "fs", split_axis=0, concat_axis=1, tiled=True),
        lax.all_to_all(up_new, "fs", split_axis=0, concat_axis=1, tiled=True),
    )
    down_out = lax.all_to_all(
        down_weight.astype(jnp.bfloat16), "fs", split_axis=0, concat_axis=2, tiled=True
    )
    tok_rows, top = routes.shape
    capacity = min(tok_rows, max(2, 3 * tok_rows * top // (2 * fs_count)))
    flat = routes.reshape(-1)
    count = flat.shape[0]
    hits = (flat[:, None] == jnp.arange(fs_count, dtype=jnp.int32)[None, :]).astype(jnp.int32)
    ranks = jnp.sum((jnp.cumsum(hits, axis=0) - 1) * hits, axis=1)
    slots = flat * capacity + ranks
    source = jnp.full((fs_count * capacity,), count, jnp.int32)
    source = source.at[slots].set(jnp.arange(count, dtype=jnp.int32))
    filled = (source < count)[:, None]
    row_of = jnp.minimum(source // top, tok_rows - 1)
    whole = lax.all_gather(tokens, "tp", axis=1, tiled=True)
    normed = normalize(whole)
    packed = jnp.where(filled, normed[row_of], jnp.zeros((), jnp.bfloat16))
    arrived = lax.all_to_all(
        packed.reshape(fs_count, capacity, -1), "fs", split_axis=0, concat_axis=0, tiled=True
    )
    arrived = arrived.reshape(fs_count * capacity, -1)
    gate_act = jnp.dot(arrived, gate_out[0], preferred_element_type=jnp.float32)
    up_act = jnp.dot(arrived, up_out[0], preferred_element_type=jnp.float32)
    hidden = (jax.nn.silu(gate_act) * up_act).astype(jnp.bfloat16)
    slot_rows = hidden.shape[0]
    unit_rows = down_out.shape[1]
    hidden_all = lax.all_gather(hidden, "tp", axis=1, tiled=True)
    column_block = lax.all_to_all(
        down_out[0].reshape(unit_rows, tp_count, -1), "tp", split_axis=1, concat_axis=0, tiled=True
    )
    column_block = column_block.reshape(tp_count, unit_rows, -1)
    hidden_blocks = hidden_all.reshape(slot_rows, tp_count, unit_rows)
    partial_value = jnp.einsum(
        "sju,jud->sjd", hidden_blocks, column_block, preferred_element_type=jnp.float32
    ).astype(jnp.bfloat16)
    expert_out = jnp.sum(partial_value, axis=1, dtype=jnp.float32).astype(jnp.bfloat16)
    returned = lax.all_to_all(
        expert_out.reshape(fs_count, capacity, -1), "fs", split_axis=0, concat_axis=0, tiled=True
    )
    returned = returned.reshape(fs_count * capacity, -1)
    picked = returned[slots].reshape(tok_rows, top, -1)
    share = route_weight / jnp.sum(route_weight, axis=1, keepdims=True)
    mixed = jnp.sum(share[:, :, None] * picked.astype(jnp.float32), axis=1).astype(jnp.bfloat16)
    return (gate_out, up_out, down_out, mixed)


MESH = pl.DeviceIdType.MESH
VMEM_BYTES = 67043328


def flip(index, mask):
    other = index
    bit = 1
    while bit <= mask:
        if mask & bit:
            other = other + (1 - 2 * lax.rem(lax.div(index, bit), 2)) * bit
        bit *= 2
    return other


def serve_kernel(
    fs, tp, cap,
    routes_ref, rw_ref, gain_ref, tokens_hbm, gw_hbm, uw_hbm, dw_hbm,
    gat, upw, dn, r, picks_ref, share_ref,
    tokens_ref, gw, uw, dw, gsend, usend, dsend,
    psend, x, n, h, wd, y,
    load_sem,
    w_s, w_r, p_s, p_r, xf_s, xf_r, h_s, h_r, wd_s, wd_r, y_s, y_r, own_sem,
):
    me = lax.axis_index("fs")
    mt = lax.axis_index("tp")
    toks, cols = tokens_ref.shape
    rows = gw.shape[1]
    units = gw.shape[2]
    each = cols // rows
    slots = fs * cap
    order = [i for k in range(fs // 2) for i in (fs - 1 - k, fs // 2 - 1 - k) if i]
    torder = list(range(1, tp))

    loads = [
        pltpu.make_async_copy(src, dst, load_sem.at[k])
        for k, (src, dst) in enumerate(
            ((gw_hbm, gw), (uw_hbm, uw), (dw_hbm, dw), (tokens_hbm, tokens_ref))
        )
    ]
    for load in loads[3:] + loads[:3]:
        load.start()

    barrier = pltpu.get_barrier_semaphore()
    for i in order:
        pl.semaphore_signal(barrier, inc=1, device_id=(flip(me, i), mt), device_id_type=MESH)
    for j in torder:
        pl.semaphore_signal(barrier, inc=1, device_id=(me, flip(mt, j)), device_id_type=MESH)

    first, second = routes_ref[0:1, :], routes_ref[1:2, :]
    expert = lax.broadcasted_iota(jnp.int32, (fs, toks), 0)
    member = (expert == first) | (expert == second)
    earlier = lax.broadcasted_iota(jnp.int32, (toks, toks), 0) < lax.broadcasted_iota(
        jnp.int32, (toks, toks), 1
    )
    rank = jnp.dot(
        jnp.where(member, 1.0, 0.0).astype(jnp.bfloat16),
        jnp.where(earlier, 1.0, 0.0).astype(jnp.bfloat16),
        preferred_element_type=jnp.float32,
    )
    rank = jnp.where(member, rank, -1.0)
    place = lax.broadcasted_iota(jnp.int32, (cap, toks), 0).astype(jnp.float32)
    loads[3].wait()
    tokens = tokens_ref[...]
    hits = []
    for e in range(fs):
        hit = jnp.where(place == rank[e:e + 1, :], 1.0, 0.0)
        psend[e] = jnp.dot(
            hit.astype(jnp.bfloat16), tokens, preferred_element_type=jnp.float32
        ).astype(jnp.bfloat16)
        hits.append(hit)
    x[mt, me] = psend[me]

    pl.semaphore_wait(barrier, fs - 1 + tp - 1)

    sends = []

    def send(src, dst, s, d, device):
        copy = pltpu.make_async_remote_copy(
            src_ref=src, dst_ref=dst, send_sem=s, recv_sem=d, device_id=device, device_id_type=MESH
        )
        copy.start()
        sends.append(copy)
        return copy

    dispatched = {}
    for i in order:
        peer = flip(me, i)
        dispatched[i] = send(psend.at[peer], x.at[mt, me], p_s.at[i], p_r.at[i], (peer, mt))

    gain = jnp.broadcast_to(gain_ref[...], (units, rows)).T
    placed = {}
    owns = []
    for k, (raw, buf, dst) in enumerate(((gw, gsend, gat), (uw, usend, upw), (dw, dsend, dn))):
        loads[k].wait()
        for e in range(fs):
            buf[e] = (gain * raw[e] if k < 2 else raw[e]).astype(jnp.bfloat16)
        for i in order:
            peer = flip(me, i)
            target = dst.at[me] if k < 2 else dst.at[:, pl.ds(pl.multiple_of(me * rows, rows), rows)]
            placed[k, i] = send(buf.at[peer], target, w_s.at[k, i], w_r.at[k, i], (peer, mt))
        target = dst.at[me] if k < 2 else dst.at[:, pl.ds(pl.multiple_of(me * rows, rows), rows)]
        own = pltpu.make_async_copy(buf.at[me], target, own_sem.at[k])
        own.start()
        owns.append(own)
        if k == 0:
            forwards = []
            for j in torder:
                forwards.append(
                    send(x.at[mt, me], x.at[mt, me], xf_s.at[0, j], xf_r.at[0, j], (me, flip(mt, j)))
                )

    for i in reversed(order):
        dispatched[i].wait_recv()
        peer = flip(me, i)
        for j in torder:
            forwards.append(
                send(x.at[mt, peer], x.at[mt, peer], xf_s.at[i, j], xf_r.at[i, j], (me, flip(mt, j)))
            )
    for k, named in enumerate((first, second)):
        picked = jnp.concatenate([jnp.where(named == e, hits[e], 0.0) for e in range(fs)], axis=0)
        picks_ref[k] = picked.T.astype(jnp.bfloat16)
        weight = rw_ref[k:k + 1, :] / (rw_ref[0:1, :] + rw_ref[1:2, :])
        share_ref[k] = jnp.broadcast_to(weight, (toks, toks)).T

    for copy in forwards:
        copy.wait_recv()

    for s in range(fs):
        total = jnp.zeros((cap, 1), jnp.float32)
        for j in range(tp):
            value = x[j, s].astype(jnp.float32)
            total = total + jnp.sum(value * value, axis=-1, keepdims=True)
        scale = lax.rsqrt(total / (tp * cols) + 1e-06)
        for j in range(tp):
            n[j, s] = (x[j, s].astype(jnp.float32) * scale).astype(jnp.bfloat16)

    acts = []
    for k, dst in enumerate((gat, upw)):
        owns[k].wait()
        for i in order:
            placed[k, i].wait_recv()
        act = jnp.zeros((slots, units), jnp.float32)
        for j in range(tp):
            act = act + jnp.dot(
                n[j].reshape(slots, cols),
                dst[j * each:(j + 1) * each].reshape(cols, units),
                preferred_element_type=jnp.float32,
            )
        acts.append(act)
    hidden = acts[0] / (1.0 + jnp.exp(-acts[0])) * acts[1]
    h[mt] = hidden.astype(jnp.bfloat16)
    shared = [send(h.at[mt], h.at[mt], h_s.at[j], h_r.at[j], (me, flip(mt, j))) for j in torder]

    moves = []
    for i in [0] + order:
        if i == 0:
            owns[2].wait()
        else:
            placed[2, i].wait_recv()
        piece = flip(me, i)
        owner, part = lax.div(piece, each), lax.rem(piece, each)
        block = dn.at[:, pl.ds(pl.multiple_of(piece * rows, rows), rows)]
        stays = pltpu.make_async_copy(block, wd.at[mt, part], wd_r.at[mt, part])
        goes = pltpu.make_async_remote_copy(
            src_ref=block, dst_ref=wd.at[mt, part], send_sem=wd_s.at[i], recv_sem=wd_r.at[mt, part],
            device_id=(me, owner), device_id_type=MESH,
        )
        pl.when(owner == mt)(stays.start)
        pl.when(owner != mt)(goes.start)
        moves.append((owner, goes))
    for copy in shared:
        copy.wait_recv()
    for j in range(tp):
        for part in range(each):
            pltpu.make_async_copy(wd.at[j, part], wd.at[j, part], wd_r.at[j, part]).wait()
    for part in range(each):
        result = jnp.zeros((slots, rows), jnp.float32)
        for j in range(tp):
            term = jnp.dot(h[j], wd[j, part], preferred_element_type=jnp.float32)
            result = result + term.astype(jnp.bfloat16).astype(jnp.float32)
        y[:, :, part * rows:(part + 1) * rows] = result.astype(jnp.bfloat16).reshape(fs, cap, rows)
    returned = []
    for i in order:
        peer = flip(me, i)
        returned.append(send(y.at[peer], r.at[me], y_s.at[i], y_r.at[i], (peer, mt)))
    r[me] = y[me]

    for copy in returned:
        copy.wait_recv()
    for copy in sends:
        copy.wait_send()
    for owner, goes in moves:
        pl.when(owner != mt)(goes.wait_send)


def mix_kernel(gat, upw, dn, r, picks_ref, share_ref, gate_hbm, up_hbm, down_hbm, mixed_hbm, mixed, sem):
    outs = [
        pltpu.make_async_copy(src, dst, sem.at[k])
        for k, (src, dst) in enumerate(
            ((gat, gate_hbm), (upw, up_hbm), (dn, down_hbm), (mixed, mixed_hbm))
        )
    ]
    for copy in outs[:3]:
        copy.start()
    fs, cap, cols = r.shape
    back = r[...].reshape(fs * cap, cols)
    total = jnp.zeros(mixed.shape, jnp.float32)
    for k in range(2):
        term = jnp.dot(picks_ref[k], back, preferred_element_type=jnp.float32)
        total = total + share_ref[k][:, 0:1] * term
    mixed[...] = total.astype(jnp.bfloat16)
    outs[3].start()
    for copy in outs:
        copy.wait()


def fused(tokens, routes, route_weight, gain, gate_weight, up_weight, down_weight):
    fs = lax.axis_size("fs")
    tp = lax.axis_size("tp")
    toks, cols = tokens.shape
    top = routes.shape[1]
    cap = capacity_of(toks, top, fs)
    rows, units = gate_weight.shape[1:]
    slots = fs * cap
    bf, f32 = jnp.bfloat16, jnp.float32
    hbm, vmem = pl.BlockSpec(memory_space=pltpu.HBM), pl.BlockSpec(memory_space=pltpu.VMEM)
    dma = pltpu.SemaphoreType.DMA
    kept = 2 * (3 * fs * rows * units + slots * cols + top * toks * slots) + 4 * top * toks * toks
    landed = pl.pallas_call(
        functools.partial(serve_kernel, fs, tp, cap),
        out_shape=(
            pltpu.VMEM((fs, rows, units), bf),
            pltpu.VMEM((fs, rows, units), bf),
            pltpu.VMEM((units, fs * rows), bf),
            pltpu.VMEM((fs, cap, cols), bf),
            pltpu.VMEM((top, toks, slots), bf),
            pltpu.VMEM((top, toks, toks), f32),
        ),
        in_specs=[vmem] * 3 + [hbm] * 4,
        out_specs=(vmem,) * 6,
        scratch_shapes=[
            pltpu.VMEM((toks, cols), bf),
            pltpu.VMEM((fs, rows, units), f32),
            pltpu.VMEM((fs, rows, units), f32),
            pltpu.VMEM((fs, units, rows), f32),
            pltpu.VMEM((fs, rows, units), bf),
            pltpu.VMEM((fs, rows, units), bf),
            pltpu.VMEM((fs, units, rows), bf),
            pltpu.VMEM((fs, cap, cols), bf),
            pltpu.VMEM((tp, fs, cap, cols), bf),
            pltpu.VMEM((tp, fs, cap, cols), bf),
            pltpu.VMEM((tp, slots, units), bf),
            pltpu.VMEM((tp, cols // rows, units, rows), bf),
            pltpu.VMEM((fs, cap, cols), bf),
            dma((4,)),
            dma((3, fs)), dma((3, fs)), dma((fs,)), dma((fs,)),
            dma((fs, tp)), dma((fs, tp)), dma((tp,)), dma((tp,)),
            dma((fs,)), dma((tp, cols // rows)), dma((fs,)), dma((fs,)), dma((3,)),
        ],
        compiler_params=pltpu.CompilerParams(
            collective_id=0, has_side_effects=True, vmem_limit_bytes=VMEM_BYTES - kept - 2**16
        ),
        name="serve",
    )(routes.T, route_weight.T, gain.reshape(1, -1), tokens, gate_weight, up_weight, down_weight)
    gate, up, down, mixed = pl.pallas_call(
        mix_kernel,
        out_shape=(
            jax.ShapeDtypeStruct((fs, rows, units), bf),
            jax.ShapeDtypeStruct((fs, rows, units), bf),
            jax.ShapeDtypeStruct((units, fs * rows), bf),
            jax.ShapeDtypeStruct((toks, cols), bf),
        ),
        in_specs=[vmem] * 6,
        out_specs=(hbm,) * 4,
        scratch_shapes=[pltpu.VMEM((toks, cols), bf), dma((4,))],
        compiler_params=pltpu.CompilerParams(vmem_limit_bytes=16 * 2**20),
        name="mix",
    )(*landed)
    return (
        gate.reshape(1, fs * rows, units),
        up.reshape(1, fs * rows, units),
        down[None],
        mixed,
    )


def capacity_of(tok_rows, top, fs_count):
    return min(tok_rows, max(2, 3 * tok_rows * top // (2 * fs_count)))


def one_kernel(fs, tp, toks, top, experts, rows, units, cols):
    cap = capacity_of(toks, top, fs)
    powers = fs & (fs - 1) == 0 and tp & (tp - 1) == 0
    small = fs <= 16 and tp <= 8 and top == 2 and experts == fs
    tiled = cap % 16 == 0 and rows % 128 == 0 and units % 128 == 0 and toks % 128 == 0
    return powers and small and tiled and cols % rows == 0 and cols % 128 == 0


def program(*args):
    tokens, routes, gate_weight = args[0], args[1], args[4]
    experts, rows, units = gate_weight.shape
    if one_kernel(
        lax.axis_size("fs"), lax.axis_size("tp"), tokens.shape[0], routes.shape[1],
        experts, rows, units, tokens.shape[1],
    ):
        return fused(*args)
    return local(*args)


def solution(mesh):
    in_specs = (
        P("fs", "tp"),
        P("fs", None),
        P("fs", None),
        P("fs"),
        P(None, "fs", "tp"),
        P(None, "fs", "tp"),
        P(None, "tp", "fs"),
    )
    out_specs = (P("fs", None, "tp"), P("fs", None, "tp"), P("fs", "tp", None), P("fs", "tp"))
    return jax.shard_map(program, mesh=mesh, in_specs=in_specs, out_specs=out_specs, check_vma=False)
```

profile of v0, /device:TPU:0, one launch (start us, length us, event | category | flops | bytes accessed | tf_op | source)
XLA Modules:
  0.0 67.1 jit_solution(7278470508980664177)
XLA Ops:
  0.6 65.2 %serve.1 = (bf16[8,256,128]{2,1,0:T(8,128)(2,1)S(1)}, bf16[8,256,128]{2,1,0:T(8,128)(2,1)S(1)}, bf16[128,2048]{1,0:T(8,128)(2,1)S(1)}, bf16[8,48,512]{2,1,0:T(8,...) custom-call(s32[2,128]{1,0:T(2,128)} %bitcast.6, f32[2,128]{1,0:T(2,128)} %bitcast.7, ...), custom_call_target="tpu_custom_call" | custom-call | tf_op jit(solution)/shard_map/serve/pallas_call | solution.py:302
  65.9 1.3 %mix.1 = (bf16[8,256,128]{2,1,0:T(8,128)(2,1)}, bf16[8,256,128]{2,1,0:T(8,128)(2,1)}, bf16[128,2048]{1,0:T(8,128)(2,1)}, bf16[128,512]{1,0:T(8,128)(2,1)}) custom-call(bf16[8,256,128]{2,1,0:T(8,128)(2,1)S(1)} %get-tuple-element.14.gat, bf16[8,256,128]{2,1,0:T(8,128)(2,1)S(1)} %get-tuple-element.15.upw, bf16[128,2048]{1,0:T(8,128)(2,1)S(1)} %get-tuple-element.16.dn, ...), custom_call_target="tpu_custom_call" | custom-call | tf_op jit(solution)/shard_map/mix/pallas_call | solution.py:338
where the time goes:
time: 67.3 us; the launch traced here: 67.1 us
  Pallas kernels  66.5 us (99%)
    pallas_call x1, Pallas kernels, fused(): pl.pallas_call(functools.partial(serve_kernel, fs, tp, cap), out_shape=(p...  65.2 us

commit v1 on v0

--- a/solution.py
+++ b/solution.py
@@ -101,7 +101,10 @@
     units = gw.shape[2]
     each = cols // rows
     slots = fs * cap
+    side = lax.div(me, fs // 2)
     order = [i for k in range(fs // 2) for i in (fs - 1 - k, fs // 2 - 1 - k) if i]
+    near = [i for i in order if i < fs // 2]
+    far = [i for i in order if i >= fs // 2]
     torder = list(range(1, tp))
 
     loads = [
@@ -114,10 +117,12 @@
         load.start()
 
     barrier = pltpu.get_barrier_semaphore()
-    for i in order:
-        pl.semaphore_signal(barrier, inc=1, device_id=(flip(me, i), mt), device_id_type=MESH)
-    for j in torder:
-        pl.semaphore_signal(barrier, inc=1, device_id=(me, flip(mt, j)), device_id_type=MESH)
+    for i in range(fs):
+        for j in range(tp):
+            if i or j:
+                pl.semaphore_signal(
+                    barrier, inc=1, device_id=(flip(me, i), flip(mt, j)), device_id_type=MESH
+                )
 
     first, second = routes_ref[0:1, :], routes_ref[1:2, :]
     expert = lax.broadcasted_iota(jnp.int32, (fs, toks), 0)
@@ -143,7 +148,7 @@
         hits.append(hit)
     x[mt, me] = psend[me]
 
-    pl.semaphore_wait(barrier, fs - 1 + tp - 1)
+    pl.semaphore_wait(barrier, fs * tp - 1)
 
     sends = []
 
@@ -167,7 +172,7 @@
         loads[k].wait()
         for e in range(fs):
             buf[e] = (gain * raw[e] if k < 2 else raw[e]).astype(jnp.bfloat16)
-        for i in order:
+        for i in order if k < 2 else near + far:
             peer = flip(me, i)
             target = dst.at[me] if k < 2 else dst.at[:, pl.ds(pl.multiple_of(me * rows, rows), rows)]
             placed[k, i] = send(buf.at[peer], target, w_s.at[k, i], w_r.at[k, i], (peer, mt))
@@ -205,65 +210,85 @@
             total = total + jnp.sum(value * value, axis=-1, keepdims=True)
         scale = lax.rsqrt(total / (tp * cols) + 1e-06)
         for j in range(tp):
-            n[j, s] = (x[j, s].astype(jnp.float32) * scale).astype(jnp.bfloat16)
+            normed = (x[j, s].astype(jnp.float32) * scale).astype(jnp.bfloat16)
+            for part in range(each):
+                n[j * each + part, s * cap:(s + 1) * cap] = normed[:, part * rows:(part + 1) * rows]
 
     acts = []
     for k, dst in enumerate((gat, upw)):
-        owns[k].wait()
-        for i in order:
-            placed[k, i].wait_recv()
         act = jnp.zeros((slots, units), jnp.float32)
-        for j in range(tp):
-            act = act + jnp.dot(
-                n[j].reshape(slots, cols),
-                dst[j * each:(j + 1) * each].reshape(cols, units),
-                preferred_element_type=jnp.float32,
-            )
+        for i in [0] + order:
+            if i == 0:
+                owns[k].wait()
+            else:
+                placed[k, i].wait_recv()
+            piece = flip(me, i)
+            act = act + jnp.dot(n[piece], dst[piece], preferred_element_type=jnp.float32)
         acts.append(act)
     hidden = acts[0] / (1.0 + jnp.exp(-acts[0])) * acts[1]
     h[mt] = hidden.astype(jnp.bfloat16)
     shared = [send(h.at[mt], h.at[mt], h_s.at[j], h_r.at[j], (me, flip(mt, j))) for j in torder]
 
     moves = []
-    for i in [0] + order:
-        if i == 0:
-            owns[2].wait()
-        else:
-            placed[2, i].wait_recv()
-        piece = flip(me, i)
-        owner, part = lax.div(piece, each), lax.rem(piece, each)
-        block = dn.at[:, pl.ds(pl.multiple_of(piece * rows, rows), rows)]
-        stays = pltpu.make_async_copy(block, wd.at[mt, part], wd_r.at[mt, part])
-        goes = pltpu.make_async_remote_copy(
-            src_ref=block, dst_ref=wd.at[mt, part], send_sem=wd_s.at[i], recv_sem=wd_r.at[mt, part],
-            device_id=(me, owner), device_id_type=MESH,
-        )
-        pl.when(owner == mt)(stays.start)
-        pl.when(owner != mt)(goes.start)
-        moves.append((owner, goes))
+
+    def gather(masks):
+        for i in masks:
+            if i == 0:
+                owns[2].wait()
+            else:
+                placed[2, i].wait_recv()
+            piece = flip(me, i)
+            owner, part = lax.rem(piece, tp), lax.div(piece, tp)
+            block = dn.at[:, pl.ds(pl.multiple_of(piece * rows, rows), rows)]
+            stays = pltpu.make_async_copy(block, wd.at[mt, part], wd_r.at[mt, part])
+            goes = pltpu.make_async_remote_copy(
+                src_ref=block, dst_ref=wd.at[mt, part], send_sem=wd_s.at[i],
+                recv_sem=wd_r.at[mt, part], device_id=(me, owner), device_id_type=MESH,
+            )
+            pl.when(owner == mt)(stays.start)
+            pl.when(owner != mt)(goes.start)
+            moves.append((owner != mt, goes))
+
+    def give_back(late):
+        for q in range(each // 2):
+            part = (1 - side if late else side) * (each // 2) + q
+            for j in range(tp):
+                pltpu.make_async_copy(wd.at[j, part], wd.at[j, part], wd_r.at[j, part]).wait()
+            result = jnp.zeros((slots, rows), jnp.float32)
+            for j in range(tp):
+                term = jnp.dot(h[j], wd[j, part], preferred_element_type=jnp.float32)
+                result = result + term.astype(jnp.bfloat16).astype(jnp.float32)
+            v = late * (each // 2) + q
+            y[v] = result.astype(jnp.bfloat16).reshape(fs, cap, rows)
+            piece = part * tp + mt
+            home, slot = lax.div(piece, each), lax.rem(piece, each)
+            for i in order:
+                peer = flip(me, i)
+                send(y.at[v, peer], r.at[slot, me], y_s.at[v, i], y_r.at[i, slot], (peer, home))
+            stays = pltpu.make_async_copy(y.at[v, me], r.at[slot, me], y_r.at[0, slot])
+            goes = pltpu.make_async_remote_copy(
+                src_ref=y.at[v, me], dst_ref=r.at[slot, me], send_sem=y_s.at[v, 0],
+                recv_sem=y_r.at[0, slot], device_id=(me, home), device_id_type=MESH,
+            )
+            pl.when(home == mt)(stays.start)
+            pl.when(home != mt)(goes.start)
+            moves.append((home != mt, goes))
+
+    gather([0] + near)
     for copy in shared:
         copy.wait_recv()
-    for j in range(tp):
-        for part in range(each):
-            pltpu.make_async_copy(wd.at[j, part], wd.at[j, part], wd_r.at[j, part]).wait()
-    for part in range(each):
-        result = jnp.zeros((slots, rows), jnp.float32)
-        for j in range(tp):
-            term = jnp.dot(h[j], wd[j, part], preferred_element_type=jnp.float32)
-            result = result + term.astype(jnp.bfloat16).astype(jnp.float32)
-        y[:, :, part * rows:(part + 1) * rows] = result.astype(jnp.bfloat16).reshape(fs, cap, rows)
-    returned = []
-    for i in order:
-        peer = flip(me, i)
-        returned.append(send(y.at[peer], r.at[me], y_s.at[i], y_r.at[i], (peer, mt)))
-    r[me] = y[me]
-
-    for copy in returned:
-        copy.wait_recv()
+    give_back(0)
+    gather(far)
+    give_back(1)
+
+    for i in [0] + order:
+        for slot in range(each):
+            landed = r.at[slot, flip(me, i)]
+            pltpu.make_async_copy(landed, landed, y_r.at[i, slot]).wait()
     for copy in sends:
         copy.wait_send()
-    for owner, goes in moves:
-        pl.when(owner != mt)(goes.wait_send)
+    for away, goes in moves:
+        pl.when(away)(goes.wait_send)
 
 
 def mix_kernel(gat, upw, dn, r, picks_ref, share_ref, gate_hbm, up_hbm, down_hbm, mixed_hbm, mixed, sem):
@@ -275,13 +300,14 @@
     ]
     for copy in outs[:3]:
         copy.start()
-    fs, cap, cols = r.shape
-    back = r[...].reshape(fs * cap, cols)
-    total = jnp.zeros(mixed.shape, jnp.float32)
-    for k in range(2):
-        term = jnp.dot(picks_ref[k], back, preferred_element_type=jnp.float32)
-        total = total + share_ref[k][:, 0:1] * term
-    mixed[...] = total.astype(jnp.bfloat16)
+    each, fs, cap, rows = r.shape
+    for slot in range(each):
+        back = r[slot].reshape(fs * cap, rows)
+        total = jnp.zeros((mixed.shape[0], rows), jnp.float32)
+        for k in range(2):
+            term = jnp.dot(picks_ref[k], back, preferred_element_type=jnp.float32)
+            total = total + share_ref[k][:, 0:1] * term
+        mixed[:, slot * rows:(slot + 1) * rows] = total.astype(jnp.bfloat16)
     outs[3].start()
     for copy in outs:
         copy.wait()
@@ -294,6 +320,7 @@
     top = routes.shape[1]
     cap = capacity_of(toks, top, fs)
     rows, units = gate_weight.shape[1:]
+    each = cols // rows
     slots = fs * cap
     bf, f32 = jnp.bfloat16, jnp.float32
     hbm, vmem = pl.BlockSpec(memory_space=pltpu.HBM), pl.BlockSpec(memory_space=pltpu.VMEM)
@@ -305,7 +332,7 @@
             pltpu.VMEM((fs, rows, units), bf),
             pltpu.VMEM((fs, rows, units), bf),
             pltpu.VMEM((units, fs * rows), bf),
-            pltpu.VMEM((fs, cap, cols), bf),
+            pltpu.VMEM((each, fs, cap, rows), bf),
             pltpu.VMEM((top, toks, slots), bf),
             pltpu.VMEM((top, toks, toks), f32),
         ),
@@ -321,14 +348,14 @@
             pltpu.VMEM((fs, units, rows), bf),
             pltpu.VMEM((fs, cap, cols), bf),
             pltpu.VMEM((tp, fs, cap, cols), bf),
-            pltpu.VMEM((tp, fs, cap, cols), bf),
+            pltpu.VMEM((fs, slots, rows), bf),
             pltpu.VMEM((tp, slots, units), bf),
-            pltpu.VMEM((tp, cols // rows, units, rows), bf),
-            pltpu.VMEM((fs, cap, cols), bf),
+            pltpu.VMEM((tp, each, units, rows), bf),
+            pltpu.VMEM((each, fs, cap, rows), bf),
             dma((4,)),
             dma((3, fs)), dma((3, fs)), dma((fs,)), dma((fs,)),
             dma((fs, tp)), dma((fs, tp)), dma((tp,)), dma((tp,)),
-            dma((fs,)), dma((tp, cols // rows)), dma((fs,)), dma((fs,)), dma((3,)),
+            dma((fs,)), dma((tp, each)), dma((each, fs)), dma((fs, each)), dma((3,)),
         ],
         compiler_params=pltpu.CompilerParams(
             collective_id=0, has_side_effects=True, vmem_limit_bytes=VMEM_BYTES - kept - 2**16
@@ -366,7 +393,7 @@
     powers = fs & (fs - 1) == 0 and tp & (tp - 1) == 0
     small = fs <= 16 and tp <= 8 and top == 2 and experts == fs
     tiled = cap % 16 == 0 and rows % 128 == 0 and units % 128 == 0 and toks % 128 == 0
-    return powers and small and tiled and cols % rows == 0 and cols % 128 == 0
+    return powers and small and tiled and cols % (2 * rows) == 0 and fs * rows == tp * cols
 
 
 def program(*args):

time: 67.3 us -> 70.4 us (1.046)
  Pallas kernels: 66.5 us -> 69.6 us
    pallas_call x1, Pallas kernels: 65.2 us -> 68.4 us  [fused(): pl.pallas_call(functools.partial(serve_kernel, fs, tp, cap), out_shape=(p...]
where the time goes in v1:
time: 70.4 us; the launch traced here: 70.3 us
  Pallas kernels  69.6 us (99%)
    pallas_call x1, Pallas kernels, fused(): pl.pallas_call(functools.partial(serve_kernel, fs, tp, cap), out_shape=(p...  68.4 us

profile of v1, /device:TPU:0, one launch (start us, length us, event | category | flops | bytes accessed | tf_op | source)
XLA Modules:
  0.0 70.3 jit_solution(10175521441564740613)
XLA Ops:
  0.6 68.4 %serve.1 = (bf16[8,256,128]{2,1,0:T(8,128)(2,1)S(1)}, bf16[8,256,128]{2,1,0:T(8,128)(2,1)S(1)}, bf16[128,2048]{1,0:T(8,128)(2,1)S(1)}, bf16[2,8,48,256]{3,2,1,0:...) custom-call(s32[2,128]{1,0:T(2,128)} %bitcast.6, f32[2,128]{1,0:T(2,128)} %bitcast.7, ...), custom_call_target="tpu_custom_call" | custom-call | tf_op jit(solution)/shard_map/serve/pallas_call | solution.py:329
  69.0 1.2 %mix.1 = (bf16[8,256,128]{2,1,0:T(8,128)(2,1)}, bf16[8,256,128]{2,1,0:T(8,128)(2,1)}, bf16[128,2048]{1,0:T(8,128)(2,1)}, bf16[128,512]{1,0:T(8,128)(2,1)}) custom-call(bf16[8,256,128]{2,1,0:T(8,128)(2,1)S(1)} %get-tuple-element.14.gat, bf16[8,256,128]{2,1,0:T(8,128)(2,1)S(1)} %get-tuple-element.15.upw, bf16[128,2048]{1,0:T(8,128)(2,1)S(1)} %get-tuple-element.16.dn, ...), custom_call_target="tpu_custom_call" | custom-call | tf_op jit(solution)/shard_map/mix/pallas_call | solution.py:365

commit v2 on v1

--- a/solution.py
+++ b/solution.py
@@ -90,9 +90,9 @@
     routes_ref, rw_ref, gain_ref, tokens_hbm, gw_hbm, uw_hbm, dw_hbm,
     gat, upw, dn, r, picks_ref, share_ref,
     tokens_ref, gw, uw, dw, gsend, usend, dsend,
-    psend, x, n, h, wd, y,
+    psend, fsend, ftoks, rsend, froutes, x, n, h, wd, y,
     load_sem,
-    w_s, w_r, p_s, p_r, xf_s, xf_r, h_s, h_r, wd_s, wd_r, y_s, y_r, own_sem,
+    w_s, w_r, t_s, t_r, p_s, p_r, xf_s, xf_r, h_s, h_r, wd_s, wd_r, y_s, y_r, own_sem,
 ):
     me = lax.axis_index("fs")
     mt = lax.axis_index("tp")
@@ -101,11 +101,15 @@
     units = gw.shape[2]
     each = cols // rows
     slots = fs * cap
-    side = lax.div(me, fs // 2)
-    order = [i for k in range(fs // 2) for i in (fs - 1 - k, fs // 2 - 1 - k) if i]
-    near = [i for i in order if i < fs // 2]
-    far = [i for i in order if i >= fs // 2]
-    torder = list(range(1, tp))
+    half = fs // 2
+    side = lax.div(me, half)
+    across = flip(me, half)
+    outer = (me < fs // 4) | (me >= fs - fs // 4)
+    near = list(range(half - 1, 0, -1))
+    far = list(range(fs - 1, half - 1, -1))
+    order = [i for pair in zip(far, near + [0]) for i in pair if i]
+    direct = [1] + list(range(2, tp, 2))
+    relayed = list(range(2, tp, 2))
 
     loads = [
         pltpu.make_async_copy(src, dst, load_sem.at[k])
@@ -119,89 +123,159 @@
     barrier = pltpu.get_barrier_semaphore()
     for i in range(fs):
         for j in range(tp):
-            if i or j:
+            if (i == 0) != (j == 0):
                 pl.semaphore_signal(
                     barrier, inc=1, device_id=(flip(me, i), flip(mt, j)), device_id_type=MESH
                 )
 
-    first, second = routes_ref[0:1, :], routes_ref[1:2, :]
-    expert = lax.broadcasted_iota(jnp.int32, (fs, toks), 0)
-    member = (expert == first) | (expert == second)
+    def remote(src, dst, s, d, device):
+        return pltpu.make_async_remote_copy(
+            src_ref=src, dst_ref=dst, send_sem=s, recv_sem=d, device_id=device, device_id_type=MESH
+        )
+
+    def drain(ref, sem):
+        pltpu.make_async_copy(ref, ref, sem).wait()
+
+    def send(*args):
+        copy = remote(*args)
+        copy.start()
+        return copy
+
     earlier = lax.broadcasted_iota(jnp.int32, (toks, toks), 0) < lax.broadcasted_iota(
         jnp.int32, (toks, toks), 1
     )
-    rank = jnp.dot(
-        jnp.where(member, 1.0, 0.0).astype(jnp.bfloat16),
-        jnp.where(earlier, 1.0, 0.0).astype(jnp.bfloat16),
-        preferred_element_type=jnp.float32,
-    )
-    rank = jnp.where(member, rank, -1.0)
+    earlier = jnp.where(earlier, 1.0, 0.0).astype(jnp.bfloat16)
     place = lax.broadcasted_iota(jnp.int32, (cap, toks), 0).astype(jnp.float32)
+
+    def ranks(one, two, lowest):
+        expert = lax.broadcasted_iota(jnp.int32, (fs, toks), 0) + lowest
+        member = (expert == one) | (expert == two)
+        rank = jnp.dot(
+            jnp.where(member, 1.0, 0.0).astype(jnp.bfloat16), earlier,
+            preferred_element_type=jnp.float32,
+        )
+        return jnp.where(member, rank, -1.0)
+
+    def pack(rank, rows_of, into):
+        for e in range(half):
+            hit = jnp.where(place == rank[e:e + 1, :], 1.0, 0.0).astype(jnp.bfloat16)
+            into[e] = jnp.dot(hit, rows_of, preferred_element_type=jnp.float32).astype(jnp.bfloat16)
+
+    first, second = routes_ref[0:1, :], routes_ref[1:2, :]
+    rsend[0:2, :] = routes_ref[...]
+    rank = ranks(first, second, side * half)
     loads[3].wait()
-    tokens = tokens_ref[...]
-    hits = []
-    for e in range(fs):
-        hit = jnp.where(place == rank[e:e + 1, :], 1.0, 0.0)
-        psend[e] = jnp.dot(
-            hit.astype(jnp.bfloat16), tokens, preferred_element_type=jnp.float32
-        ).astype(jnp.bfloat16)
-        hits.append(hit)
-    x[mt, me] = psend[me]
-
-    pl.semaphore_wait(barrier, fs * tp - 1)
-
-    sends = []
-
-    def send(src, dst, s, d, device):
-        copy = pltpu.make_async_remote_copy(
-            src_ref=src, dst_ref=dst, send_sem=s, recv_sem=d, device_id=device, device_id_type=MESH
-        )
-        copy.start()
-        sends.append(copy)
-        return copy
-
-    dispatched = {}
-    for i in order:
-        peer = flip(me, i)
-        dispatched[i] = send(psend.at[peer], x.at[mt, me], p_s.at[i], p_r.at[i], (peer, mt))
+    pack(rank, tokens_ref[...], psend)
+    x[mt, me] = psend[lax.rem(me, half)]
+
+    pl.semaphore_wait(barrier, fs - 1 + tp - 1)
+
+    crossing = [
+        send(rsend, froutes, t_s.at[0], t_r.at[0], (across, mt)),
+        send(tokens_ref, ftoks, t_s.at[1], t_r.at[1], (across, mt)),
+    ]
+    spread = {}
+
+    def dispatch(buf, block, base):
+        for i in near:
+            peer = flip(me, i)
+            spread[base + i] = send(
+                buf.at[lax.rem(peer, half)], x.at[mt, block], p_s.at[0], p_r.at[base + i],
+                (peer, mt),
+            )
+
+    def forward(i):
+        block = flip(me, i)
+        for j in direct:
+            send(
+                x.at[mt, block], x.at[mt, block], xf_s.at[0], xf_r.at[j, i // half], (me, flip(mt, j))
+            )
+
+    dispatch(psend, me, 0)
+    forward(0)
 
     gain = jnp.broadcast_to(gain_ref[...], (units, rows)).T
     placed = {}
     owns = []
+    held = {}
     for k, (raw, buf, dst) in enumerate(((gw, gsend, gat), (uw, usend, upw), (dw, dsend, dn))):
         loads[k].wait()
         for e in range(fs):
             buf[e] = (gain * raw[e] if k < 2 else raw[e]).astype(jnp.bfloat16)
-        for i in order if k < 2 else near + far:
+        target = dst.at[me] if k < 2 else dst.at[:, pl.ds(pl.multiple_of(me * rows, rows), rows)]
+        held[k] = []
+        for i in order:
             peer = flip(me, i)
-            target = dst.at[me] if k < 2 else dst.at[:, pl.ds(pl.multiple_of(me * rows, rows), rows)]
-            placed[k, i] = send(buf.at[peer], target, w_s.at[k, i], w_r.at[k, i], (peer, mt))
-        target = dst.at[me] if k < 2 else dst.at[:, pl.ds(pl.multiple_of(me * rows, rows), rows)]
+            arrived = (0 if k == 0 else near[0] if k == 2 and i < half else i)
+            copy = remote(buf.at[peer], target, w_s.at[k], w_r.at[k, arrived], (peer, mt))
+            placed[k, i] = copy
+            if i >= half:
+                pl.when(jnp.logical_not(outer))(copy.start)
+                held[k].append(copy)
         own = pltpu.make_async_copy(buf.at[me], target, own_sem.at[k])
         own.start()
         owns.append(own)
-        if k == 0:
-            forwards = []
-            for j in torder:
-                forwards.append(
-                    send(x.at[mt, me], x.at[mt, me], xf_s.at[0, j], xf_r.at[0, j], (me, flip(mt, j)))
-                )
-
-    for i in reversed(order):
-        dispatched[i].wait_recv()
-        peer = flip(me, i)
-        for j in torder:
-            forwards.append(
-                send(x.at[mt, peer], x.at[mt, peer], xf_s.at[i, j], xf_r.at[i, j], (me, flip(mt, j)))
-            )
+
+    def release(k):
+        def start():
+            for copy in held[k]:
+                copy.start()
+        pl.when(outer)(start)
+
+    for copy in crossing:
+        copy.wait_recv()
+    pack(ranks(froutes[0:1, :], froutes[1:2, :], side * half), ftoks[...], fsend)
+    x[mt, across] = fsend[lax.rem(me, half)]
+    dispatch(fsend, across, half)
+    forward(half)
+    for k in range(3):
+        for i in near:
+            placed[k, i].start()
+    release(0)
+    release(1)
+    for i in near:
+        spread[i].wait_recv()
+        forward(i)
+    for i in near:
+        spread[half + i].wait_recv()
+        forward(half + i)
+
+    for v in range(2):
+        first_block = pl.multiple_of((1 - side if v else side) * half, half)
+        for j in relayed:
+            landed = x.at[flip(mt, j), pl.ds(first_block, half)]
+            drain(landed, xf_r.at[j, v])
+            send(landed, landed, xf_s.at[0], xf_r.at[j + 1, v], (me, flip(mt, 1)))
+
+    def gather(masks):
+        for i in masks:
+            if i == 0:
+                owns[2].wait()
+            elif i >= half:
+                placed[2, i].wait_recv()
+            elif i == near[0]:
+                drain(dsend.at[pl.ds(0, half - 1)], w_r.at[2, i])
+            piece = flip(me, i)
+            owner, part = lax.rem(piece, tp), lax.div(piece, tp)
+            block = dn.at[:, pl.ds(pl.multiple_of(piece * rows, rows), rows)]
+            landing = wd_r.at[i // half]
+            stays = pltpu.make_async_copy(block, wd.at[mt, part], landing)
+            goes = remote(block, wd.at[mt, part], wd_s.at[0], landing, (me, owner))
+            pl.when(owner == mt)(stays.start)
+            pl.when(owner != mt)(goes.start)
+
+    rank = ranks(first, second, 0)
+    hits = [jnp.where(place == rank[e:e + 1, :], 1.0, 0.0) for e in range(fs)]
+    gather([0] + near)
     for k, named in enumerate((first, second)):
         picked = jnp.concatenate([jnp.where(named == e, hits[e], 0.0) for e in range(fs)], axis=0)
         picks_ref[k] = picked.T.astype(jnp.bfloat16)
         weight = rw_ref[k:k + 1, :] / (rw_ref[0:1, :] + rw_ref[1:2, :])
         share_ref[k] = jnp.broadcast_to(weight, (toks, toks)).T
 
-    for copy in forwards:
-        copy.wait_recv()
+    for v in range(2):
+        for j in range(1, tp, 2):
+            drain(x.at[0, pl.ds(0, half)], xf_r.at[j, v])
 
     for s in range(fs):
         total = jnp.zeros((cap, 1), jnp.float32)
@@ -214,46 +288,40 @@
             for part in range(each):
                 n[j * each + part, s * cap:(s + 1) * cap] = normed[:, part * rows:(part + 1) * rows]
 
-    acts = []
-    for k, dst in enumerate((gat, upw)):
+    def activate(k, dst):
         act = jnp.zeros((slots, units), jnp.float32)
         for i in [0] + order:
             if i == 0:
                 owns[k].wait()
-            else:
+            elif k == 1:
                 placed[k, i].wait_recv()
+            elif i == order[0]:
+                drain(dst.at[pl.ds(0, fs - 1)], w_r.at[0, 0])
             piece = flip(me, i)
             act = act + jnp.dot(n[piece], dst[piece], preferred_element_type=jnp.float32)
-        acts.append(act)
-    hidden = acts[0] / (1.0 + jnp.exp(-acts[0])) * acts[1]
-    h[mt] = hidden.astype(jnp.bfloat16)
-    shared = [send(h.at[mt], h.at[mt], h_s.at[j], h_r.at[j], (me, flip(mt, j))) for j in torder]
+        return act
+
+    gate_act = activate(0, gat)
+    gate_act = gate_act / (1.0 + jnp.exp(-gate_act))
+    up_act = activate(1, upw)
+    h[mt] = (gate_act * up_act).astype(jnp.bfloat16)
+    shared = {j: send(h.at[mt], h.at[mt], h_s.at[0], h_r.at[j], (me, flip(mt, j))) for j in direct}
+    release(2)
+    for j in relayed:
+        shared[j].wait_recv()
+        source = flip(mt, j)
+        shared[j + 1] = send(
+            h.at[source], h.at[source], h_s.at[0], h_r.at[j + 1], (me, flip(mt, 1))
+        )
 
     moves = []
 
-    def gather(masks):
-        for i in masks:
-            if i == 0:
-                owns[2].wait()
-            else:
-                placed[2, i].wait_recv()
-            piece = flip(me, i)
-            owner, part = lax.rem(piece, tp), lax.div(piece, tp)
-            block = dn.at[:, pl.ds(pl.multiple_of(piece * rows, rows), rows)]
-            stays = pltpu.make_async_copy(block, wd.at[mt, part], wd_r.at[mt, part])
-            goes = pltpu.make_async_remote_copy(
-                src_ref=block, dst_ref=wd.at[mt, part], send_sem=wd_s.at[i],
-                recv_sem=wd_r.at[mt, part], device_id=(me, owner), device_id_type=MESH,
-            )
-            pl.when(owner == mt)(stays.start)
-            pl.when(owner != mt)(goes.start)
-            moves.append((owner != mt, goes))
-
     def give_back(late):
+        waiting = []
+        first_part = (1 - side if late else side) * (each // 2)
+        drain(wd.at[:, pl.ds(0, each // 2)], wd_r.at[late])
         for q in range(each // 2):
-            part = (1 - side if late else side) * (each // 2) + q
-            for j in range(tp):
-                pltpu.make_async_copy(wd.at[j, part], wd.at[j, part], wd_r.at[j, part]).wait()
+            part = first_part + q
             result = jnp.zeros((slots, rows), jnp.float32)
             for j in range(tp):
                 term = jnp.dot(h[j], wd[j, part], preferred_element_type=jnp.float32)
@@ -262,31 +330,42 @@
             y[v] = result.astype(jnp.bfloat16).reshape(fs, cap, rows)
             piece = part * tp + mt
             home, slot = lax.div(piece, each), lax.rem(piece, each)
-            for i in order:
+            for i in far + near:
                 peer = flip(me, i)
-                send(y.at[v, peer], r.at[slot, me], y_s.at[v, i], y_r.at[i, slot], (peer, home))
-            stays = pltpu.make_async_copy(y.at[v, me], r.at[slot, me], y_r.at[0, slot])
-            goes = pltpu.make_async_remote_copy(
-                src_ref=y.at[v, me], dst_ref=r.at[slot, me], send_sem=y_s.at[v, 0],
-                recv_sem=y_r.at[0, slot], device_id=(me, home), device_id_type=MESH,
-            )
+                copy = remote(y.at[v, peer], r.at[slot, me], y_s.at[0], y_r.at[0], (peer, home))
+                if late or i < half:
+                    copy.start()
+                else:
+                    pl.when(jnp.logical_not(outer))(copy.start)
+                    waiting.append(copy)
+            stays = pltpu.make_async_copy(y.at[v, me], r.at[slot, me], y_r.at[0])
+            goes = remote(y.at[v, me], r.at[slot, me], y_s.at[1 + v], y_r.at[0], (me, home))
             pl.when(home == mt)(stays.start)
             pl.when(home != mt)(goes.start)
             moves.append((home != mt, goes))
-
-    gather([0] + near)
-    for copy in shared:
-        copy.wait_recv()
-    give_back(0)
+        return waiting
+
+    for j, copy in shared.items():
+        if j % 2:
+            copy.wait_recv()
+    held[3] = give_back(0)
     gather(far)
+    release(3)
     give_back(1)
 
-    for i in [0] + order:
-        for slot in range(each):
-            landed = r.at[slot, flip(me, i)]
-            pltpu.make_async_copy(landed, landed, y_r.at[i, slot]).wait()
-    for copy in sends:
+    drain(r, y_r.at[0])
+    for copy in crossing:
         copy.wait_send()
+    for k, buf in enumerate((gsend, usend, dsend)):
+        drain(buf.at[pl.ds(0, fs - 1)], w_s.at[k])
+    for _ in range(2):
+        drain(psend.at[pl.ds(0, half - 1)], p_s.at[0])
+    for _ in range(tp - 1):
+        drain(x.at[0], xf_s.at[0])
+    drain(h.at[pl.ds(0, tp - 1)], h_s.at[0])
+    for _ in range(tp - 1):
+        drain(wd.at[0], wd_s.at[0])
+    drain(y.at[:, pl.ds(0, fs - 1)], y_s.at[0])
     for away, goes in moves:
         pl.when(away)(goes.wait_send)
 
@@ -346,16 +425,20 @@
             pltpu.VMEM((fs, rows, units), bf),
             pltpu.VMEM((fs, rows, units), bf),
             pltpu.VMEM((fs, units, rows), bf),
-            pltpu.VMEM((fs, cap, cols), bf),
+            pltpu.VMEM((fs // 2, cap, cols), bf),
+            pltpu.VMEM((fs // 2, cap, cols), bf),
+            pltpu.VMEM((toks, cols), bf),
+            pltpu.VMEM((8, toks), jnp.int32),
+            pltpu.VMEM((8, toks), jnp.int32),
             pltpu.VMEM((tp, fs, cap, cols), bf),
             pltpu.VMEM((fs, slots, rows), bf),
             pltpu.VMEM((tp, slots, units), bf),
             pltpu.VMEM((tp, each, units, rows), bf),
             pltpu.VMEM((each, fs, cap, rows), bf),
             dma((4,)),
-            dma((3, fs)), dma((3, fs)), dma((fs,)), dma((fs,)),
-            dma((fs, tp)), dma((fs, tp)), dma((tp,)), dma((tp,)),
-            dma((fs,)), dma((tp, each)), dma((each, fs)), dma((fs, each)), dma((3,)),
+            dma((3,)), dma((3, fs)), dma((2,)), dma((2,)), dma((1,)), dma((fs,)),
+            dma((1,)), dma((tp, 2)), dma((1,)), dma((tp,)),
+            dma((1,)), dma((2,)), dma((1 + each,)), dma((1,)), dma((3,)),
         ],
         compiler_params=pltpu.CompilerParams(
             collective_id=0, has_side_effects=True, vmem_limit_bytes=VMEM_BYTES - kept - 2**16
@@ -390,7 +473,7 @@
 
 def one_kernel(fs, tp, toks, top, experts, rows, units, cols):
     cap = capacity_of(toks, top, fs)
-    powers = fs & (fs - 1) == 0 and tp & (tp - 1) == 0
+    powers = fs & (fs - 1) == 0 and tp & (tp - 1) == 0 and fs >= 4 and tp >= 2
     small = fs <= 16 and tp <= 8 and top == 2 and experts == fs
     tiled = cap % 16 == 0 and rows % 128 == 0 and units % 128 == 0 and toks % 128 == 0
     return powers and small and tiled and cols % (2 * rows) == 0 and fs * rows == tp * cols

time: 70.4 us -> 59.1 us (0.84)
  Pallas kernels: 69.6 us -> 58.2 us
    pallas_call x1, Pallas kernels: 68.4 us -> 57 us  [fused(): pl.pallas_call(functools.partial(serve_kernel, fs, tp, cap), out_shape=(p...]
where the time goes in v2:
time: 59.1 us; the launch traced here: 58.9 us
  Pallas kernels  58.2 us (98%)
  between operations  0.64 us (1%)
    pallas_call x1, Pallas kernels, fused(): pl.pallas_call(functools.partial(serve_kernel, fs, tp, cap), out_shape=(p...  57 us
    pallas_call x1, Pallas kernels, fused(): pl.pallas_call(mix_kernel, out_shape=(jax.ShapeDtypeStruct((fs, rows, uni...  1.22 us

profile of v2, /device:TPU:0, one launch (start us, length us, event | category | flops | bytes accessed | tf_op | source)
XLA Modules:
  0.0 58.9 jit_solution(13271597003720373566)
XLA Ops:
  0.6 57.0 %serve.1 = (bf16[8,256,128]{2,1,0:T(8,128)(2,1)S(1)}, bf16[8,256,128]{2,1,0:T(8,128)(2,1)S(1)}, bf16[128,2048]{1,0:T(8,128)(2,1)S(1)}, bf16[2,8,48,256]{3,2,1,0:...) custom-call(s32[2,128]{1,0:T(2,128)} %bitcast.6, f32[2,128]{1,0:T(2,128)} %bitcast.7, ...), custom_call_target="tpu_custom_call" | custom-call | tf_op jit(solution)/shard_map/serve/pallas_call | solution.py:408
  57.7 1.2 %mix.1 = (bf16[8,256,128]{2,1,0:T(8,128)(2,1)}, bf16[8,256,128]{2,1,0:T(8,128)(2,1)}, bf16[128,2048]{1,0:T(8,128)(2,1)}, bf16[128,512]{1,0:T(8,128)(2,1)}) custom-call(bf16[8,256,128]{2,1,0:T(8,128)(2,1)S(1)} %get-tuple-element.14.gat, bf16[8,256,128]{2,1,0:T(8,128)(2,1)S(1)} %get-tuple-element.15.upw, bf16[128,2048]{1,0:T(8,128)(2,1)S(1)} %get-tuple-element.16.dn, ...), custom_call_target="tpu_custom_call" | custom-call | tf_op jit(solution)/shard_map/mix/pallas_call | solution.py:448

commit v3 on v2

--- a/solution.py
+++ b/solution.py
@@ -92,7 +92,7 @@
     tokens_ref, gw, uw, dw, gsend, usend, dsend,
     psend, fsend, ftoks, rsend, froutes, x, n, h, wd, y,
     load_sem,
-    w_s, w_r, t_s, t_r, p_s, p_r, xf_s, xf_r, h_s, h_r, wd_s, wd_r, y_s, y_r, own_sem,
+    w_s, w_r, t_s, t_r, p_s, p_r, xf_s, xf_r, h_s, h_r, wd_s, wd_r, y_s, y_r, own_sem, met,
 ):
     me = lax.axis_index("fs")
     mt = lax.axis_index("tp")
@@ -103,11 +103,14 @@
     slots = fs * cap
     half = fs // 2
     side = lax.div(me, half)
-    across = flip(me, half)
+    bridge = half | half // 2
+    across = flip(me, bridge)
     outer = (me < fs // 4) | (me >= fs - fs // 4)
     near = list(range(half - 1, 0, -1))
-    far = list(range(fs - 1, half - 1, -1))
-    order = [i for pair in zip(far, near + [0]) for i in pair if i]
+    far = [flip(me, i) for i in range(fs - 1, half - 1, -1)]
+    homeward = [jnp.where(side == 1, q, fs - 1 - q) for q in range(half)]
+    links = [(i, 0) for i in [1 << b for b in range(half.bit_length() - 1)] + [bridge]]
+    links += [(0, 1 << b) for b in range(tp.bit_length() - 1)]
     direct = [1] + list(range(2, tp, 2))
     relayed = list(range(2, tp, 2))
 
@@ -121,12 +124,14 @@
         load.start()
 
     barrier = pltpu.get_barrier_semaphore()
-    for i in range(fs):
-        for j in range(tp):
-            if (i == 0) != (j == 0):
-                pl.semaphore_signal(
-                    barrier, inc=1, device_id=(flip(me, i), flip(mt, j)), device_id_type=MESH
-                )
+
+    def greet(sem):
+        for i, j in links:
+            pl.semaphore_signal(
+                sem, inc=1, device_id=(flip(me, i), flip(mt, j)), device_id_type=MESH
+            )
+
+    greet(barrier)
 
     def remote(src, dst, s, d, device):
         return pltpu.make_async_remote_copy(
@@ -168,12 +173,16 @@
     pack(rank, tokens_ref[...], psend)
     x[mt, me] = psend[lax.rem(me, half)]
 
-    pl.semaphore_wait(barrier, fs - 1 + tp - 1)
-
+    pl.semaphore_wait(barrier, len(links))
+    greet(met.at[0])
     crossing = [
         send(rsend, froutes, t_s.at[0], t_r.at[0], (across, mt)),
         send(tokens_ref, ftoks, t_s.at[1], t_r.at[1], (across, mt)),
     ]
+    pl.semaphore_wait(met.at[0], len(links))
+    greet(met.at[1])
+    pl.semaphore_wait(met.at[1], len(links))
+
     spread = {}
 
     def dispatch(buf, block, base):
@@ -184,15 +193,15 @@
                 (peer, mt),
             )
 
-    def forward(i):
-        block = flip(me, i)
+    def forward(i, apart):
+        block = flip(me, i ^ bridge if apart else i)
         for j in direct:
             send(
-                x.at[mt, block], x.at[mt, block], xf_s.at[0], xf_r.at[j, i // half], (me, flip(mt, j))
+                x.at[mt, block], x.at[mt, block], xf_s.at[0], xf_r.at[j, apart], (me, flip(mt, j))
             )
 
     dispatch(psend, me, 0)
-    forward(0)
+    forward(0, 0)
 
     gain = jnp.broadcast_to(gain_ref[...], (units, rows)).T
     placed = {}
@@ -204,41 +213,42 @@
             buf[e] = (gain * raw[e] if k < 2 else raw[e]).astype(jnp.bfloat16)
         target = dst.at[me] if k < 2 else dst.at[:, pl.ds(pl.multiple_of(me * rows, rows), rows)]
         held[k] = []
-        for i in order:
+        base = 0 if k == 0 else 2 if k == 1 else 3 + half
+        for i in near:
             peer = flip(me, i)
-            arrived = (0 if k == 0 else near[0] if k == 2 and i < half else i)
-            copy = remote(buf.at[peer], target, w_s.at[k], w_r.at[k, arrived], (peer, mt))
-            placed[k, i] = copy
-            if i >= half:
-                pl.when(jnp.logical_not(outer))(copy.start)
-                held[k].append(copy)
+            placed[k, i] = remote(buf.at[peer], target, w_s.at[k], w_r.at[base], (peer, mt))
+            if k == 0:
+                placed[k, i].start()
+        for v, peer in enumerate(far):
+            arrived = base + 1 + (v if k else 0)
+            copy = remote(buf.at[peer], target, w_s.at[k], w_r.at[arrived], (peer, mt))
+            pl.when(jnp.logical_not(outer))(copy.start)
+            held[k].append((outer, copy))
         own = pltpu.make_async_copy(buf.at[me], target, own_sem.at[k])
         own.start()
         owns.append(own)
 
     def release(k):
-        def start():
-            for copy in held[k]:
-                copy.start()
-        pl.when(outer)(start)
+        for when, copy in held[k]:
+            pl.when(when)(copy.start)
 
     for copy in crossing:
         copy.wait_recv()
     pack(ranks(froutes[0:1, :], froutes[1:2, :], side * half), ftoks[...], fsend)
     x[mt, across] = fsend[lax.rem(me, half)]
     dispatch(fsend, across, half)
-    forward(half)
-    for k in range(3):
+    forward(0, 1)
+    for k in (1, 2):
         for i in near:
             placed[k, i].start()
     release(0)
     release(1)
     for i in near:
         spread[i].wait_recv()
-        forward(i)
+        forward(i, 0)
     for i in near:
         spread[half + i].wait_recv()
-        forward(half + i)
+        forward(i, 1)
 
     for v in range(2):
         first_block = pl.multiple_of((1 - side if v else side) * half, half)
@@ -247,18 +257,17 @@
             drain(landed, xf_r.at[j, v])
             send(landed, landed, xf_s.at[0], xf_r.at[j + 1, v], (me, flip(mt, 1)))
 
-    def gather(masks):
-        for i in masks:
-            if i == 0:
+    def gather(apart):
+        for v in range(half):
+            if apart:
+                drain(dsend.at[0], w_r.at[4 + half + v])
+            elif v == 0:
                 owns[2].wait()
-            elif i >= half:
-                placed[2, i].wait_recv()
-            elif i == near[0]:
-                drain(dsend.at[pl.ds(0, half - 1)], w_r.at[2, i])
-            piece = flip(me, i)
+                drain(dsend.at[pl.ds(0, half - 1)], w_r.at[3 + half])
+            piece = far[v] if apart else flip(me, v)
             owner, part = lax.rem(piece, tp), lax.div(piece, tp)
             block = dn.at[:, pl.ds(pl.multiple_of(piece * rows, rows), rows)]
-            landing = wd_r.at[i // half]
+            landing = wd_r.at[apart]
             stays = pltpu.make_async_copy(block, wd.at[mt, part], landing)
             goes = remote(block, wd.at[mt, part], wd_s.at[0], landing, (me, owner))
             pl.when(owner == mt)(stays.start)
@@ -266,7 +275,6 @@
 
     rank = ranks(first, second, 0)
     hits = [jnp.where(place == rank[e:e + 1, :], 1.0, 0.0) for e in range(fs)]
-    gather([0] + near)
     for k, named in enumerate((first, second)):
         picked = jnp.concatenate([jnp.where(named == e, hits[e], 0.0) for e in range(fs)], axis=0)
         picks_ref[k] = picked.T.astype(jnp.bfloat16)
@@ -289,20 +297,22 @@
                 n[j * each + part, s * cap:(s + 1) * cap] = normed[:, part * rows:(part + 1) * rows]
 
     def activate(k, dst):
+        base = 0 if k == 0 else 2
+        owns[k].wait()
+        drain(dst.at[pl.ds(0, half - 1)], w_r.at[base])
+        pieces = [me] + [flip(me, i) for i in near] + far
         act = jnp.zeros((slots, units), jnp.float32)
-        for i in [0] + order:
-            if i == 0:
-                owns[k].wait()
-            elif k == 1:
-                placed[k, i].wait_recv()
-            elif i == order[0]:
-                drain(dst.at[pl.ds(0, fs - 1)], w_r.at[0, 0])
-            piece = flip(me, i)
+        for v, piece in enumerate(pieces):
+            if k == 0 and v == half:
+                drain(dst.at[pl.ds(0, half)], w_r.at[base + 1])
+            if k == 1 and v >= half:
+                drain(dst.at[0], w_r.at[base + 1 + v - half])
             act = act + jnp.dot(n[piece], dst[piece], preferred_element_type=jnp.float32)
         return act
 
     gate_act = activate(0, gat)
     gate_act = gate_act / (1.0 + jnp.exp(-gate_act))
+    gather(0)
     up_act = activate(1, upw)
     h[mt] = (gate_act * up_act).astype(jnp.bfloat16)
     shared = {j: send(h.at[mt], h.at[mt], h_s.at[0], h_r.at[j], (me, flip(mt, j))) for j in direct}
@@ -330,14 +340,16 @@
             y[v] = result.astype(jnp.bfloat16).reshape(fs, cap, rows)
             piece = part * tp + mt
             home, slot = lax.div(piece, each), lax.rem(piece, each)
-            for i in far + near:
-                peer = flip(me, i)
+            for peer in homeward:
                 copy = remote(y.at[v, peer], r.at[slot, me], y_s.at[0], y_r.at[0], (peer, home))
-                if late or i < half:
+                if late:
                     copy.start()
                 else:
                     pl.when(jnp.logical_not(outer))(copy.start)
-                    waiting.append(copy)
+                    waiting.append((outer, copy))
+            for i in near:
+                peer = flip(me, i)
+                send(y.at[v, peer], r.at[slot, me], y_s.at[0], y_r.at[0], (peer, home))
             stays = pltpu.make_async_copy(y.at[v, me], r.at[slot, me], y_r.at[0])
             goes = remote(y.at[v, me], r.at[slot, me], y_s.at[1 + v], y_r.at[0], (me, home))
             pl.when(home == mt)(stays.start)
@@ -349,7 +361,7 @@
         if j % 2:
             copy.wait_recv()
     held[3] = give_back(0)
-    gather(far)
+    gather(1)
     release(3)
     give_back(1)
 
@@ -436,9 +448,10 @@
             pltpu.VMEM((tp, each, units, rows), bf),
             pltpu.VMEM((each, fs, cap, rows), bf),
             dma((4,)),
-            dma((3,)), dma((3, fs)), dma((2,)), dma((2,)), dma((1,)), dma((fs,)),
+            dma((3,)), dma((fs + 4,)), dma((2,)), dma((2,)), dma((1,)), dma((fs,)),
             dma((1,)), dma((tp, 2)), dma((1,)), dma((tp,)),
             dma((1,)), dma((2,)), dma((1 + each,)), dma((1,)), dma((3,)),
+            pltpu.SemaphoreType.REGULAR((2,)),
         ],
         compiler_params=pltpu.CompilerParams(
             collective_id=0, has_side_effects=True, vmem_limit_bytes=VMEM_BYTES - kept - 2**16

time: 59.1 us -> 57.5 us (0.973)
  Pallas kernels: 58.2 us -> 56.7 us
    pallas_call x1, Pallas kernels: 57 us -> 55.4 us  [fused(): pl.pallas_call(functools.partial(serve_kernel, fs, tp, cap), out_shape=(p...]
where the time goes in v3:
time: 57.5 us; the launch traced here: 57.3 us
  Pallas kernels  56.7 us (99%)
  between operations  0.64 us (1%)
    pallas_call x1, Pallas kernels, fused(): pl.pallas_call(functools.partial(serve_kernel, fs, tp, cap), out_shape=(p...  55.4 us
    pallas_call x1, Pallas kernels, fused(): pl.pallas_call(mix_kernel, out_shape=(jax.ShapeDtypeStruct((fs, rows, uni...  1.22 us

profile of v3, /device:TPU:0, one launch (start us, length us, event | category | flops | bytes accessed | tf_op | source)
XLA Modules:
  0.0 57.3 jit_solution(11226813473660420345)
XLA Ops:
  0.6 55.4 %serve.1 = (bf16[8,256,128]{2,1,0:T(8,128)(2,1)S(1)}, bf16[8,256,128]{2,1,0:T(8,128)(2,1)S(1)}, bf16[128,2048]{1,0:T(8,128)(2,1)S(1)}, bf16[2,8,48,256]{3,2,1,0:...) custom-call(s32[2,128]{1,0:T(2,128)} %bitcast.6, f32[2,128]{1,0:T(2,128)} %bitcast.7, ...), custom_call_target="tpu_custom_call" | custom-call | tf_op jit(solution)/shard_map/serve/pallas_call | solution.py:420
  56.1 1.2 %mix.1 = (bf16[8,256,128]{2,1,0:T(8,128)(2,1)}, bf16[8,256,128]{2,1,0:T(8,128)(2,1)}, bf16[128,2048]{1,0:T(8,128)(2,1)}, bf16[128,512]{1,0:T(8,128)(2,1)}) custom-call(bf16[8,256,128]{2,1,0:T(8,128)(2,1)S(1)} %get-tuple-element.14.gat, bf16[8,256,128]{2,1,0:T(8,128)(2,1)S(1)} %get-tuple-element.15.upw, bf16[128,2048]{1,0:T(8,128)(2,1)S(1)} %get-tuple-element.16.dn, ...), custom_call_target="tpu_custom_call" | custom-call | tf_op jit(solution)/shard_map/mix/pallas_call | solution.py:461

commit v4 on v3

--- a/solution.py
+++ b/solution.py
@@ -92,7 +92,7 @@
     tokens_ref, gw, uw, dw, gsend, usend, dsend,
     psend, fsend, ftoks, rsend, froutes, x, n, h, wd, y,
     load_sem,
-    w_s, w_r, t_s, t_r, p_s, p_r, xf_s, xf_r, h_s, h_r, wd_s, wd_r, y_s, y_r, own_sem, met,
+    out, w_r, t_r, p_r, xf_r, h_r, wd_r, y_s, y_r, met,
 ):
     me = lax.axis_index("fs")
     mt = lax.axis_index("tp")
@@ -176,20 +176,18 @@
     pl.semaphore_wait(barrier, len(links))
     greet(met.at[0])
     crossing = [
-        send(rsend, froutes, t_s.at[0], t_r.at[0], (across, mt)),
-        send(tokens_ref, ftoks, t_s.at[1], t_r.at[1], (across, mt)),
+        send(rsend, froutes, out.at[0], t_r.at[0], (across, mt)),
+        send(tokens_ref, ftoks, out.at[0], t_r.at[1], (across, mt)),
     ]
     pl.semaphore_wait(met.at[0], len(links))
     greet(met.at[1])
     pl.semaphore_wait(met.at[1], len(links))
 
-    spread = {}
-
     def dispatch(buf, block, base):
         for i in near:
             peer = flip(me, i)
-            spread[base + i] = send(
-                buf.at[lax.rem(peer, half)], x.at[mt, block], p_s.at[0], p_r.at[base + i],
+            send(
+                buf.at[lax.rem(peer, half)], x.at[mt, block], out.at[0], p_r.at[base],
                 (peer, mt),
             )
 
@@ -197,7 +195,7 @@
         block = flip(me, i ^ bridge if apart else i)
         for j in direct:
             send(
-                x.at[mt, block], x.at[mt, block], xf_s.at[0], xf_r.at[j, apart], (me, flip(mt, j))
+                x.at[mt, block], x.at[mt, block], out.at[0], xf_r.at[j - 1, apart], (me, flip(mt, j))
             )
 
     dispatch(psend, me, 0)
@@ -205,7 +203,6 @@
 
     gain = jnp.broadcast_to(gain_ref[...], (units, rows)).T
     placed = {}
-    owns = []
     held = {}
     for k, (raw, buf, dst) in enumerate(((gw, gsend, gat), (uw, usend, upw), (dw, dsend, dn))):
         loads[k].wait()
@@ -216,60 +213,61 @@
         base = 0 if k == 0 else 2 if k == 1 else 3 + half
         for i in near:
             peer = flip(me, i)
-            placed[k, i] = remote(buf.at[peer], target, w_s.at[k], w_r.at[base], (peer, mt))
+            placed[k, i] = remote(buf.at[peer], target, out.at[0], w_r.at[base], (peer, mt))
             if k == 0:
                 placed[k, i].start()
         for v, peer in enumerate(far):
             arrived = base + 1 + (v if k else 0)
-            copy = remote(buf.at[peer], target, w_s.at[k], w_r.at[arrived], (peer, mt))
+            copy = remote(buf.at[peer], target, out.at[0], w_r.at[arrived], (peer, mt))
             pl.when(jnp.logical_not(outer))(copy.start)
             held[k].append((outer, copy))
-        own = pltpu.make_async_copy(buf.at[me], target, own_sem.at[k])
-        own.start()
-        owns.append(own)
+        if k < 2:
+            dst[me] = buf[me]
+        else:
+            dst[:, pl.ds(pl.multiple_of(me * rows, rows), rows)] = buf[me]
 
     def release(k):
         for when, copy in held[k]:
-            pl.when(when)(copy.start)
+            if when is True:
+                copy.start()
+            else:
+                pl.when(when)(copy.start)
 
     for copy in crossing:
         copy.wait_recv()
     pack(ranks(froutes[0:1, :], froutes[1:2, :], side * half), ftoks[...], fsend)
     x[mt, across] = fsend[lax.rem(me, half)]
-    dispatch(fsend, across, half)
+    dispatch(fsend, across, 1)
     forward(0, 1)
-    for k in (1, 2):
+    for k in (2, 1):
         for i in near:
             placed[k, i].start()
     release(0)
     release(1)
-    for i in near:
-        spread[i].wait_recv()
-        forward(i, 0)
-    for i in near:
-        spread[half + i].wait_recv()
-        forward(i, 1)
+    for apart in range(2):
+        drain(psend.at[pl.ds(0, half - 1)], p_r.at[apart])
+        for i in near:
+            forward(i, apart)
 
     for v in range(2):
         first_block = pl.multiple_of((1 - side if v else side) * half, half)
         for j in relayed:
             landed = x.at[flip(mt, j), pl.ds(first_block, half)]
-            drain(landed, xf_r.at[j, v])
-            send(landed, landed, xf_s.at[0], xf_r.at[j + 1, v], (me, flip(mt, 1)))
+            drain(landed, xf_r.at[j - 1, v])
+            send(landed, landed, out.at[0], xf_r.at[j, v], (me, flip(mt, 1)))
 
     def gather(apart):
         for v in range(half):
             if apart:
                 drain(dsend.at[0], w_r.at[4 + half + v])
             elif v == 0:
-                owns[2].wait()
                 drain(dsend.at[pl.ds(0, half - 1)], w_r.at[3 + half])
             piece = far[v] if apart else flip(me, v)
             owner, part = lax.rem(piece, tp), lax.div(piece, tp)
             block = dn.at[:, pl.ds(pl.multiple_of(piece * rows, rows), rows)]
             landing = wd_r.at[apart]
             stays = pltpu.make_async_copy(block, wd.at[mt, part], landing)
-            goes = remote(block, wd.at[mt, part], wd_s.at[0], landing, (me, owner))
+            goes = remote(block, wd.at[mt, part], out.at[0], landing, (me, owner))
             pl.when(owner == mt)(stays.start)
             pl.when(owner != mt)(goes.start)
 
@@ -283,7 +281,7 @@
 
     for v in range(2):
         for j in range(1, tp, 2):
-            drain(x.at[0, pl.ds(0, half)], xf_r.at[j, v])
+            drain(x.at[0, pl.ds(0, half)], xf_r.at[j - 1, v])
 
     for s in range(fs):
         total = jnp.zeros((cap, 1), jnp.float32)
@@ -298,7 +296,6 @@
 
     def activate(k, dst):
         base = 0 if k == 0 else 2
-        owns[k].wait()
         drain(dst.at[pl.ds(0, half - 1)], w_r.at[base])
         pieces = [me] + [flip(me, i) for i in near] + far
         act = jnp.zeros((slots, units), jnp.float32)
@@ -315,13 +312,13 @@
     gather(0)
     up_act = activate(1, upw)
     h[mt] = (gate_act * up_act).astype(jnp.bfloat16)
-    shared = {j: send(h.at[mt], h.at[mt], h_s.at[0], h_r.at[j], (me, flip(mt, j))) for j in direct}
+    shared = {j: send(h.at[mt], h.at[mt], out.at[0], h_r.at[j - 1], (me, flip(mt, j))) for j in direct}
     release(2)
     for j in relayed:
         shared[j].wait_recv()
         source = flip(mt, j)
         shared[j + 1] = send(
-            h.at[source], h.at[source], h_s.at[0], h_r.at[j + 1], (me, flip(mt, 1))
+            h.at[source], h.at[source], out.at[0], h_r.at[j], (me, flip(mt, 1))
         )
 
     moves = []
@@ -341,17 +338,16 @@
             piece = part * tp + mt
             home, slot = lax.div(piece, each), lax.rem(piece, each)
             for peer in homeward:
-                copy = remote(y.at[v, peer], r.at[slot, me], y_s.at[0], y_r.at[0], (peer, home))
+                copy = remote(y.at[v, peer], r.at[slot, me], out.at[0], y_r.at[0], (peer, home))
                 if late:
                     copy.start()
                 else:
-                    pl.when(jnp.logical_not(outer))(copy.start)
-                    waiting.append((outer, copy))
+                    waiting.append((True, copy))
             for i in near:
                 peer = flip(me, i)
-                send(y.at[v, peer], r.at[slot, me], y_s.at[0], y_r.at[0], (peer, home))
+                send(y.at[v, peer], r.at[slot, me], out.at[0], y_r.at[0], (peer, home))
             stays = pltpu.make_async_copy(y.at[v, me], r.at[slot, me], y_r.at[0])
-            goes = remote(y.at[v, me], r.at[slot, me], y_s.at[1 + v], y_r.at[0], (me, home))
+            goes = remote(y.at[v, me], r.at[slot, me], y_s.at[v], y_r.at[0], (me, home))
             pl.when(home == mt)(stays.start)
             pl.when(home != mt)(goes.start)
             moves.append((home != mt, goes))
@@ -369,15 +365,15 @@
     for copy in crossing:
         copy.wait_send()
     for k, buf in enumerate((gsend, usend, dsend)):
-        drain(buf.at[pl.ds(0, fs - 1)], w_s.at[k])
+        drain(buf.at[pl.ds(0, fs - 1)], out.at[0])
     for _ in range(2):
-        drain(psend.at[pl.ds(0, half - 1)], p_s.at[0])
+        drain(psend.at[pl.ds(0, half - 1)], out.at[0])
     for _ in range(tp - 1):
-        drain(x.at[0], xf_s.at[0])
-    drain(h.at[pl.ds(0, tp - 1)], h_s.at[0])
+        drain(x.at[0], out.at[0])
+    drain(h.at[pl.ds(0, tp - 1)], out.at[0])
     for _ in range(tp - 1):
-        drain(wd.at[0], wd_s.at[0])
-    drain(y.at[:, pl.ds(0, fs - 1)], y_s.at[0])
+        drain(wd.at[0], out.at[0])
+    drain(y.at[:, pl.ds(0, fs - 1)], out.at[0])
     for away, goes in moves:
         pl.when(away)(goes.wait_send)
 
@@ -448,9 +444,8 @@
             pltpu.VMEM((tp, each, units, rows), bf),
             pltpu.VMEM((each, fs, cap, rows), bf),
             dma((4,)),
-            dma((3,)), dma((fs + 4,)), dma((2,)), dma((2,)), dma((1,)), dma((fs,)),
-            dma((1,)), dma((tp, 2)), dma((1,)), dma((tp,)),
-            dma((1,)), dma((2,)), dma((1 + each,)), dma((1,)), dma((3,)),
+            dma((1,)), dma((fs + 4,)), dma((2,)), dma((2,)), dma((tp - 1, 2)), dma((tp - 1,)),
+            dma((2,)), dma((each,)), dma((1,)),
             pltpu.SemaphoreType.REGULAR((2,)),
         ],
         compiler_params=pltpu.CompilerParams(

time: 57.5 us -> 57.3 us (level)
  no operation moved by 1% of the time
where the time goes in v4:
time: 57.3 us; the launch traced here: 57.2 us
  Pallas kernels  56.5 us (99%)
  between operations  0.64 us (1%)
    pallas_call x1, Pallas kernels, fused(): pl.pallas_call(functools.partial(serve_kernel, fs, tp, cap), out_shape=(p...  55.3 us
    pallas_call x1, Pallas kernels, fused(): pl.pallas_call(mix_kernel, out_shape=(jax.ShapeDtypeStruct((fs, rows, uni...  1.22 us

profile of v4, /device:TPU:0, one launch (start us, length us, event | category | flops | bytes accessed | tf_op | source)
XLA Modules:
  0.0 57.2 jit_solution(15785375857622515205)
XLA Ops:
  0.6 55.3 %serve.1 = (bf16[8,256,128]{2,1,0:T(8,128)(2,1)S(1)}, bf16[8,256,128]{2,1,0:T(8,128)(2,1)S(1)}, bf16[128,2048]{1,0:T(8,128)(2,1)S(1)}, bf16[2,8,48,256]{3,2,1,0:...) custom-call(s32[2,128]{1,0:T(2,128)} %bitcast.6, f32[2,128]{1,0:T(2,128)} %bitcast.7, ...), custom_call_target="tpu_custom_call" | custom-call | tf_op jit(solution)/shard_map/serve/pallas_call | solution.py:416
  55.9 1.2 %mix.1 = (bf16[8,256,128]{2,1,0:T(8,128)(2,1)}, bf16[8,256,128]{2,1,0:T(8,128)(2,1)}, bf16[128,2048]{1,0:T(8,128)(2,1)}, bf16[128,512]{1,0:T(8,128)(2,1)}) custom-call(bf16[8,256,128]{2,1,0:T(8,128)(2,1)S(1)} %get-tuple-element.14.gat, bf16[8,256,128]{2,1,0:T(8,128)(2,1)S(1)} %get-tuple-element.15.upw, bf16[128,2048]{1,0:T(8,128)(2,1)S(1)} %get-tuple-element.16.dn, ...), custom_call_target="tpu_custom_call" | custom-call | tf_op jit(solution)/shard_map/mix/pallas_call | solution.py:456

commit v5 on v4

--- a/solution.py
+++ b/solution.py
@@ -88,11 +88,11 @@
 def serve_kernel(
     fs, tp, cap,
     routes_ref, rw_ref, gain_ref, tokens_hbm, gw_hbm, uw_hbm, dw_hbm,
-    gat, upw, dn, r, picks_ref, share_ref,
+    gat, upw, dn, r, rc, picks_ref, share_ref,
     tokens_ref, gw, uw, dw, gsend, usend, dsend,
-    psend, fsend, ftoks, rsend, froutes, x, n, h, wd, y,
+    psend, fsend, ftoks, rsend, froutes, ssend, fshares, x, n, h, wd, y, fpicks, fweights, col, whole,
     load_sem,
-    out, w_r, t_r, p_r, xf_r, h_r, wd_r, y_s, y_r, met,
+    out, w_r, t_r, p_r, xf_r, h_r, wd_r, y_s, y_r, met, c_r, m_r,
 ):
     me = lax.axis_index("fs")
     mt = lax.axis_index("tp")
@@ -131,6 +131,8 @@
                 sem, inc=1, device_id=(flip(me, i), flip(mt, j)), device_id_type=MESH
             )
 
+    r[...] = jnp.zeros(r.shape, r.dtype)
+    rc[...] = jnp.zeros(rc.shape, rc.dtype)
     greet(barrier)
 
     def remote(src, dst, s, d, device):
@@ -168,6 +170,7 @@
 
     first, second = routes_ref[0:1, :], routes_ref[1:2, :]
     rsend[0:2, :] = routes_ref[...]
+    ssend[0:2, :] = rw_ref[...] / (rw_ref[0:1, :] + rw_ref[1:2, :])
     rank = ranks(first, second, side * half)
     loads[3].wait()
     pack(rank, tokens_ref[...], psend)
@@ -177,6 +180,7 @@
     greet(met.at[0])
     crossing = [
         send(rsend, froutes, out.at[0], t_r.at[0], (across, mt)),
+        send(ssend, fshares, out.at[0], t_r.at[2], (across, mt)),
         send(tokens_ref, ftoks, out.at[0], t_r.at[1], (across, mt)),
     ]
     pl.semaphore_wait(met.at[0], len(links))
@@ -228,10 +232,7 @@
 
     def release(k):
         for when, copy in held[k]:
-            if when is True:
-                copy.start()
-            else:
-                pl.when(when)(copy.start)
+            pl.when(when)(copy.start)
 
     for copy in crossing:
         copy.wait_recv()
@@ -256,8 +257,8 @@
             drain(landed, xf_r.at[j - 1, v])
             send(landed, landed, out.at[0], xf_r.at[j, v], (me, flip(mt, 1)))
 
-    def gather(apart):
-        for v in range(half):
+    def gather(apart, steps):
+        for v in steps:
             if apart:
                 drain(dsend.at[0], w_r.at[4 + half + v])
             elif v == 0:
@@ -271,13 +272,20 @@
             pl.when(owner == mt)(stays.start)
             pl.when(owner != mt)(goes.start)
 
-    rank = ranks(first, second, 0)
-    hits = [jnp.where(place == rank[e:e + 1, :], 1.0, 0.0) for e in range(fs)]
-    for k, named in enumerate((first, second)):
-        picked = jnp.concatenate([jnp.where(named == e, hits[e], 0.0) for e in range(fs)], axis=0)
-        picks_ref[k] = picked.T.astype(jnp.bfloat16)
-        weight = rw_ref[k:k + 1, :] / (rw_ref[0:1, :] + rw_ref[1:2, :])
-        share_ref[k] = jnp.broadcast_to(weight, (toks, toks)).T
+    def choose(one, two, lowest, experts, shares, picks, weights):
+        rank = ranks(one, two, lowest)
+        hits = [jnp.where(place == rank[e:e + 1, :], 1.0, 0.0) for e in range(experts)]
+        for k, named in enumerate((one, two)):
+            picked = jnp.concatenate(
+                [jnp.where(named == e + lowest, hits[e], 0.0) for e in range(experts)], axis=0
+            )
+            picks[k] = picked.T.astype(jnp.bfloat16)
+            weights[k] = jnp.broadcast_to(shares[k:k + 1, :], (toks, toks)).T
+
+    choose(first, second, 0, fs, ssend, picks_ref, share_ref)
+    choose(
+        froutes[0:1, :], froutes[1:2, :], side * half, half, fshares, fpicks, fweights
+    )
 
     for v in range(2):
         for j in range(1, tp, 2):
@@ -309,7 +317,7 @@
 
     gate_act = activate(0, gat)
     gate_act = gate_act / (1.0 + jnp.exp(-gate_act))
-    gather(0)
+    gather(0, range(half))
     up_act = activate(1, upw)
     h[mt] = (gate_act * up_act).astype(jnp.bfloat16)
     shared = {j: send(h.at[mt], h.at[mt], out.at[0], h_r.at[j - 1], (me, flip(mt, j))) for j in direct}
@@ -324,7 +332,6 @@
     moves = []
 
     def give_back(late):
-        waiting = []
         first_part = (1 - side if late else side) * (each // 2)
         drain(wd.at[:, pl.ds(0, each // 2)], wd_r.at[late])
         for q in range(each // 2):
@@ -337,12 +344,15 @@
             y[v] = result.astype(jnp.bfloat16).reshape(fs, cap, rows)
             piece = part * tp + mt
             home, slot = lax.div(piece, each), lax.rem(piece, each)
-            for peer in homeward:
-                copy = remote(y.at[v, peer], r.at[slot, me], out.at[0], y_r.at[0], (peer, home))
-                if late:
-                    copy.start()
-                else:
-                    waiting.append((True, copy))
+            if late:
+                for peer in homeward:
+                    send(y.at[v, peer], r.at[slot, me], out.at[0], y_r.at[1], (peer, home))
+            else:
+                mine = lax.rem(me, half)
+                for i in near:
+                    peer = flip(me, i)
+                    send(y.at[v, flip(me, i ^ bridge)], col.at[q, mine], out.at[0], c_r.at[0], (peer, mt))
+                col[q, mine] = y[v, across]
             for i in near:
                 peer = flip(me, i)
                 send(y.at[v, peer], r.at[slot, me], out.at[0], y_r.at[0], (peer, home))
@@ -351,17 +361,44 @@
             pl.when(home == mt)(stays.start)
             pl.when(home != mt)(goes.start)
             moves.append((home != mt, goes))
+
+    def combine():
+        waiting = []
+        for _ in range(each // 2):
+            drain(col.at[0, pl.ds(0, half - 1)], c_r.at[0])
+        for q in range(each // 2):
+            back = col[q].reshape(half * cap, rows)
+            total = jnp.zeros((toks, rows), jnp.float32)
+            for k in range(2):
+                term = jnp.dot(fpicks[k], back, preferred_element_type=jnp.float32)
+                total = total + fweights[k][:, 0:1] * term
+            whole[q] = total.astype(jnp.bfloat16)
+            piece = (side * (each // 2) + q) * tp + mt
+            home, slot = lax.div(piece, each), lax.rem(piece, each)
+            copy = remote(whole.at[q], rc.at[slot], out.at[0], m_r.at[0], (across, home))
+            copy.start()
         return waiting
 
     for j, copy in shared.items():
         if j % 2:
             copy.wait_recv()
-    held[3] = give_back(0)
-    gather(1)
+    give_back(0)
+    gather(1, range(half))
+    held[3] = combine()
     release(3)
     give_back(1)
 
-    drain(r, y_r.at[0])
+    drain(r.at[:, pl.ds(0, half)], y_r.at[0])
+    alike = lax.div(mt, tp // 2) == side
+
+    @pl.when(alike)
+    def _():
+        drain(r.at[:, pl.ds(0, half)], y_r.at[1])
+
+    @pl.when(jnp.logical_not(alike))
+    def _():
+        drain(rc, m_r.at[0])
+
     for copy in crossing:
         copy.wait_send()
     for k, buf in enumerate((gsend, usend, dsend)):
@@ -373,12 +410,15 @@
     drain(h.at[pl.ds(0, tp - 1)], out.at[0])
     for _ in range(tp - 1):
         drain(wd.at[0], out.at[0])
-    drain(y.at[:, pl.ds(0, fs - 1)], out.at[0])
+    drain(y.at[pl.ds(0, each // 2), pl.ds(0, half - 1)], out.at[0])
+    drain(y.at[pl.ds(0, each // 2), pl.ds(0, fs - 1)], out.at[0])
+    drain(y.at[pl.ds(0, each // 2), pl.ds(0, half - 1)], out.at[0])
+    drain(whole, out.at[0])
     for away, goes in moves:
         pl.when(away)(goes.wait_send)
 
 
-def mix_kernel(gat, upw, dn, r, picks_ref, share_ref, gate_hbm, up_hbm, down_hbm, mixed_hbm, mixed, sem):
+def mix_kernel(gat, upw, dn, r, rc, picks_ref, share_ref, gate_hbm, up_hbm, down_hbm, mixed_hbm, mixed, sem):
     outs = [
         pltpu.make_async_copy(src, dst, sem.at[k])
         for k, (src, dst) in enumerate(
@@ -390,7 +430,7 @@
     each, fs, cap, rows = r.shape
     for slot in range(each):
         back = r[slot].reshape(fs * cap, rows)
-        total = jnp.zeros((mixed.shape[0], rows), jnp.float32)
+        total = rc[slot].astype(jnp.float32)
         for k in range(2):
             term = jnp.dot(picks_ref[k], back, preferred_element_type=jnp.float32)
             total = total + share_ref[k][:, 0:1] * term
@@ -412,7 +452,7 @@
     bf, f32 = jnp.bfloat16, jnp.float32
     hbm, vmem = pl.BlockSpec(memory_space=pltpu.HBM), pl.BlockSpec(memory_space=pltpu.VMEM)
     dma = pltpu.SemaphoreType.DMA
-    kept = 2 * (3 * fs * rows * units + slots * cols + top * toks * slots) + 4 * top * toks * toks
+    kept = 2 * (3 * fs * rows * units + slots * cols + toks * cols + top * toks * slots) + 4 * top * toks * toks
     landed = pl.pallas_call(
         functools.partial(serve_kernel, fs, tp, cap),
         out_shape=(
@@ -420,11 +460,12 @@
             pltpu.VMEM((fs, rows, units), bf),
             pltpu.VMEM((units, fs * rows), bf),
             pltpu.VMEM((each, fs, cap, rows), bf),
+            pltpu.VMEM((each, toks, rows), bf),
             pltpu.VMEM((top, toks, slots), bf),
             pltpu.VMEM((top, toks, toks), f32),
         ),
         in_specs=[vmem] * 3 + [hbm] * 4,
-        out_specs=(vmem,) * 6,
+        out_specs=(vmem,) * 7,
         scratch_shapes=[
             pltpu.VMEM((toks, cols), bf),
             pltpu.VMEM((fs, rows, units), f32),
@@ -438,15 +479,22 @@
             pltpu.VMEM((toks, cols), bf),
             pltpu.VMEM((8, toks), jnp.int32),
             pltpu.VMEM((8, toks), jnp.int32),
+            pltpu.VMEM((8, toks), f32),
+            pltpu.VMEM((8, toks), f32),
             pltpu.VMEM((tp, fs, cap, cols), bf),
             pltpu.VMEM((fs, slots, rows), bf),
             pltpu.VMEM((tp, slots, units), bf),
             pltpu.VMEM((tp, each, units, rows), bf),
             pltpu.VMEM((each, fs, cap, rows), bf),
+            pltpu.VMEM((top, toks, slots // 2), bf),
+            pltpu.VMEM((top, toks, toks), f32),
+            pltpu.VMEM((each // 2, fs // 2, cap, rows), bf),
+            pltpu.VMEM((each // 2, toks, rows), bf),
             dma((4,)),
-            dma((1,)), dma((fs + 4,)), dma((2,)), dma((2,)), dma((tp - 1, 2)), dma((tp - 1,)),
-            dma((2,)), dma((each,)), dma((1,)),
+            dma((1,)), dma((fs + 4,)), dma((3,)), dma((2,)), dma((tp - 1, 2)), dma((tp - 1,)),
+            dma((2,)), dma((each,)), dma((2,)),
             pltpu.SemaphoreType.REGULAR((2,)),
+            dma((1,)), dma((1,)),
         ],
         compiler_params=pltpu.CompilerParams(
             collective_id=0, has_side_effects=True, vmem_limit_bytes=VMEM_BYTES - kept - 2**16
@@ -461,7 +509,7 @@
             jax.ShapeDtypeStruct((units, fs * rows), bf),
             jax.ShapeDtypeStruct((toks, cols), bf),
         ),
-        in_specs=[vmem] * 6,
+        in_specs=[vmem] * 7,
         out_specs=(hbm,) * 4,
         scratch_shapes=[pltpu.VMEM((toks, cols), bf), dma((4,))],
         compiler_params=pltpu.CompilerParams(vmem_limit_bytes=16 * 2**20),

time: 57.3 us -> 57 us (level)
  no operation moved by 1% of the time
where the time goes in v5:
time: 57 us; the launch traced here: 56.8 us
  Pallas kernels  56.2 us (99%)
  between operations  0.64 us (1%)
    pallas_call x1, Pallas kernels, fused(): pl.pallas_call(functools.partial(serve_kernel, fs, tp, cap), out_shape=(p...  54.9 us
    pallas_call x1, Pallas kernels, fused(): pl.pallas_call(mix_kernel, out_shape=(jax.ShapeDtypeStruct((fs, rows, uni...  1.22 us

profile of v5, /device:TPU:0, one launch (start us, length us, event | category | flops | bytes accessed | tf_op | source)
XLA Modules:
  0.0 56.8 jit_solution(8917438415507123484)
XLA Ops:
  0.6 54.9 %serve.1 = (bf16[8,256,128]{2,1,0:T(8,128)(2,1)S(1)}, bf16[8,256,128]{2,1,0:T(8,128)(2,1)S(1)}, bf16[128,2048]{1,0:T(8,128)(2,1)S(1)}, bf16[2,8,48,256]{3,2,1,0:...) custom-call(s32[2,128]{1,0:T(2,128)} %bitcast.6, ...), custom_call_target="tpu_custom_call" | custom-call | tf_op jit(solution)/shard_map/serve/pallas_call | solution.py:456
  55.6 1.2 %mix.1 = (bf16[8,256,128]{2,1,0:T(8,128)(2,1)}, bf16[8,256,128]{2,1,0:T(8,128)(2,1)}, bf16[128,2048]{1,0:T(8,128)(2,1)}, bf16[128,512]{1,0:T(8,128)(2,1)}) custom-call(bf16[8,256,128]{2,1,0:T(8,128)(2,1)S(1)} %get-tuple-element.15.gat, bf16[8,256,128]{2,1,0:T(8,128)(2,1)S(1)} %get-tuple-element.16.upw, bf16[128,2048]{1,0:T(8,128)(2,1)S(1)} %get-tuple-element.17.dn, ...), custom_call_target="tpu_custom_call" | custom-call | tf_op jit(solution)/shard_map/mix/pallas_call | solution.py:504

commit v6 on v5

--- a/solution.py
+++ b/solution.py
@@ -207,7 +207,7 @@
 
     gain = jnp.broadcast_to(gain_ref[...], (units, rows)).T
     placed = {}
-    held = {}
+    held = {4: []}
     for k, (raw, buf, dst) in enumerate(((gw, gsend, gat), (uw, usend, upw), (dw, dsend, dn))):
         loads[k].wait()
         for e in range(fs):
@@ -223,7 +223,11 @@
         for v, peer in enumerate(far):
             arrived = base + 1 + (v if k else 0)
             copy = remote(buf.at[peer], target, out.at[0], w_r.at[arrived], (peer, mt))
-            pl.when(jnp.logical_not(outer))(copy.start)
+            if k < 2:
+                pl.when(jnp.logical_not(outer))(copy.start)
+            else:
+                pl.when(jnp.logical_not(outer) & (lax.rem(mt, 2) == 0))(copy.start)
+                held[4].append((jnp.logical_not(outer) & (lax.rem(mt, 2) == 1), copy))
             held[k].append((outer, copy))
         if k < 2:
             dst[me] = buf[me]
@@ -315,6 +319,7 @@
             act = act + jnp.dot(n[piece], dst[piece], preferred_element_type=jnp.float32)
         return act
 
+    release(4)
     gate_act = activate(0, gat)
     gate_act = gate_act / (1.0 + jnp.exp(-gate_act))
     gather(0, range(half))

time: 57 us -> 56.9 us (level)
  no operation moved by 1% of the time
where the time goes in v6:
time: 56.9 us; the launch traced here: 56.7 us
  Pallas kernels  56.1 us (99%)
  between operations  0.64 us (1%)
    pallas_call x1, Pallas kernels, fused(): pl.pallas_call(functools.partial(serve_kernel, fs, tp, cap), out_shape=(p...  54.9 us
    pallas_call x1, Pallas kernels, fused(): pl.pallas_call(mix_kernel, out_shape=(jax.ShapeDtypeStruct((fs, rows, uni...  1.22 us

profile of v6, /device:TPU:0, one launch (start us, length us, event | category | flops | bytes accessed | tf_op | source)
XLA Modules:
  0.0 56.7 jit_solution(16548816100013078275)
XLA Ops:
  0.6 54.9 %serve.1 = (bf16[8,256,128]{2,1,0:T(8,128)(2,1)S(1)}, bf16[8,256,128]{2,1,0:T(8,128)(2,1)S(1)}, bf16[128,2048]{1,0:T(8,128)(2,1)S(1)}, bf16[2,8,48,256]{3,2,1,0:...) custom-call(s32[2,128]{1,0:T(2,128)} %bitcast.6, ...), custom_call_target="tpu_custom_call" | custom-call | tf_op jit(solution)/shard_map/serve/pallas_call | solution.py:461
  55.5 1.2 %mix.1 = (bf16[8,256,128]{2,1,0:T(8,128)(2,1)}, bf16[8,256,128]{2,1,0:T(8,128)(2,1)}, bf16[128,2048]{1,0:T(8,128)(2,1)}, bf16[128,512]{1,0:T(8,128)(2,1)}) custom-call(bf16[8,256,128]{2,1,0:T(8,128)(2,1)S(1)} %get-tuple-element.15.gat, bf16[8,256,128]{2,1,0:T(8,128)(2,1)S(1)} %get-tuple-element.16.upw, bf16[128,2048]{1,0:T(8,128)(2,1)S(1)} %get-tuple-element.17.dn, ...), custom_call_target="tpu_custom_call" | custom-call | tf_op jit(solution)/shard_map/mix/pallas_call | solution.py:509

commit v7 on v6

--- a/solution.py
+++ b/solution.py
@@ -349,6 +349,8 @@
             y[v] = result.astype(jnp.bfloat16).reshape(fs, cap, rows)
             piece = part * tp + mt
             home, slot = lax.div(piece, each), lax.rem(piece, each)
+            peer = flip(me, near[-1])
+            send(y.at[v, peer], r.at[slot, me], out.at[0], y_r.at[0], (peer, home))
             if late:
                 for peer in homeward:
                     send(y.at[v, peer], r.at[slot, me], out.at[0], y_r.at[1], (peer, home))
@@ -358,7 +360,7 @@
                     peer = flip(me, i)
                     send(y.at[v, flip(me, i ^ bridge)], col.at[q, mine], out.at[0], c_r.at[0], (peer, mt))
                 col[q, mine] = y[v, across]
-            for i in near:
+            for i in near[:-1]:
                 peer = flip(me, i)
                 send(y.at[v, peer], r.at[slot, me], out.at[0], y_r.at[0], (peer, home))
             stays = pltpu.make_async_copy(y.at[v, me], r.at[slot, me], y_r.at[0])

time: 56.9 us -> 57 us (level)
  no operation moved by 1% of the time
where the time goes in v7:
time: 57 us; the launch traced here: 56.8 us
  Pallas kernels  56.2 us (99%)
  between operations  0.64 us (1%)
    pallas_call x1, Pallas kernels, fused(): pl.pallas_call(functools.partial(serve_kernel, fs, tp, cap), out_shape=(p...  55 us
    pallas_call x1, Pallas kernels, fused(): pl.pallas_call(mix_kernel, out_shape=(jax.ShapeDtypeStruct((fs, rows, uni...  1.22 us

profile of v7, /device:TPU:0, one launch (start us, length us, event | category | flops | bytes accessed | tf_op | source)
XLA Modules:
  0.0 56.8 jit_solution(7931442729259949145)
XLA Ops:
  0.6 55.0 %serve.1 = (bf16[8,256,128]{2,1,0:T(8,128)(2,1)S(1)}, bf16[8,256,128]{2,1,0:T(8,128)(2,1)S(1)}, bf16[128,2048]{1,0:T(8,128)(2,1)S(1)}, bf16[2,8,48,256]{3,2,1,0:...) custom-call(s32[2,128]{1,0:T(2,128)} %bitcast.6, ...), custom_call_target="tpu_custom_call" | custom-call | tf_op jit(solution)/shard_map/serve/pallas_call | solution.py:463
  55.6 1.2 %mix.1 = (bf16[8,256,128]{2,1,0:T(8,128)(2,1)}, bf16[8,256,128]{2,1,0:T(8,128)(2,1)}, bf16[128,2048]{1,0:T(8,128)(2,1)}, bf16[128,512]{1,0:T(8,128)(2,1)}) custom-call(bf16[8,256,128]{2,1,0:T(8,128)(2,1)S(1)} %get-tuple-element.15.gat, bf16[8,256,128]{2,1,0:T(8,128)(2,1)S(1)} %get-tuple-element.16.upw, bf16[128,2048]{1,0:T(8,128)(2,1)S(1)} %get-tuple-element.17.dn, ...), custom_call_target="tpu_custom_call" | custom-call | tf_op jit(solution)/shard_map/mix/pallas_call | solution.py:511
